TPU v7x, 128 devices: a whole 4x4x4 slice. The times are simulated.
128 devices in a mesh: kv: 16 (over z, x), tp: 8 (over y, core).
Axes of the slice: x: 4, y: 4, z: 4, core: 2. Of those that a mesh axis runs over, the one named last changes fastest.
Arguments:
- activations: bfloat16 [384, 2048], P(None, ('kv', 'tp')), may hold values from -6 to 6
- latent_cache: bfloat16 [24, 32768, 288], P(None, 'kv'), may hold values from -6 to 6
- lengths: int32 [24], replicated, may hold values from 8192 to 32736, as said below
- accepted: int32 [24], replicated, may hold values from 0 to 16
- parents: int32 [24, 16], replicated, may hold values from -1 to 14, as said below
- w_query_down: bfloat16 [2048, 512], P(('kv', 'tp')), may hold values from -0.125 to 0.125
- w_key_down: bfloat16 [2048, 288], P(('kv', 'tp')), may hold values from -0.125 to 0.125
- gain_input: bfloat16 [2048], P(('kv', 'tp')), may hold values from 0.099609375 to 1.8984375
- gain_query: bfloat16 [512], replicated, may hold values from 0.099609375 to 1.8984375
- gain_key: bfloat16 [256], replicated, may hold values from 0.099609375 to 1.8984375
- w_query: bfloat16 [512, 16, 288], P(None, 'tp'), as said below
- w_value: bfloat16 [16, 256, 64], replicated, may hold values from -0.375 to 0.375
- w_out: bfloat16 [1024, 2048], P('tp', 'kv'), may hold values from -1 to 1, as said below
- gain_output: bfloat16 [2048], P('kv'), may hold values from 0.099609375 to 1.8984375
Outputs:
- mixed: bfloat16 [384, 2048], P(None, 'kv')
- new_cache: bfloat16 [24, 32768, 288], P(None, 'kv')
Inputs may be any that keep to these rules, and one draw needn't show every extreme that they name: One sequence has lengths exactly 32736 and another exactly 8192; which ones varies. accepted is between 0 and 16, so the proposals' positions lie below 32768. `parents`: the parent of proposal i is -1 or a proposal with a smaller index; proposal 0 has parent -1; the proposals of exactly one sequence (which one varies) form a single chain; the other sequences' proposals form general trees. `w_query`: entries are normal with standard deviation (1536)^(-1/2) cut at six standard deviations; in the hidden draw the heads whose index is a multiple of 4 are 48 times larger. `w_out`: entries of order (1024)^(-1/2).
All inputs are finite; a program needn't handle non-finite values.
Results may differ from a plain program's by a relative error of at most 0.0096.
The roundings to bfloat16 on the way count: a program that leaves them out, or rounds other values in their place, can miss the bound.
Values may be sent and summed in bfloat16 or wider, within the bound.
No kernel may reach another device: no remote copies, remote signals or barrier semaphores. Data moves between devices by JAX's collectives and lax.ppermute only.
A program may use at most 192 MiB of HBM per device.

v0:
```python
import functools

import jax
import jax.numpy as jnp
from jax import lax
from jax.sharding import Mesh
from jax.sharding import PartitionSpec as P

D = 2048
ROPE_DIM = 32
NOPE_DIM = 64
KV_TP = ("kv_0", "kv_1", "tp_0", "tp_1")
KV = ("kv_0", "kv_1")
TP = ("tp_0", "tp_1")


epsilon = 1e-06
rope_base = 10000.0
score_after_mask = -1e30


def filled_up(lines, length):
    spare = -lines.shape[0] % length
    if not spare:
        return lines
    return jnp.concatenate([lines, jnp.zeros((spare, *lines.shape[1:]), lines.dtype)])


def copy_for_each(value, axis):
    length = lax.axis_size(axis)
    return lax.all_to_all(
        jnp.broadcast_to(value[None], (length, *value.shape)), axis, 0, 0, tiled=True
    )


def laid_out(blocks, dim):
    shape = list(blocks.shape[1:])
    shape[dim] *= blocks.shape[0]
    return jnp.moveaxis(blocks, 0, dim).reshape(shape)


def gather_axes(value, axes, dim):
    far, near = axes
    blocks = copy_for_each(copy_for_each(value, far), near)
    return laid_out(blocks.swapaxes(0, 1).reshape(-1, *value.shape), dim)


def cut_along(value, dim, length):
    before, after = (value.shape[:dim], value.shape[dim + 1 :])
    return jnp.moveaxis(value.reshape(*before, length, -1, *after), dim, 0)


def sent_and_summed(value, axis, dim):
    length = lax.axis_size(axis)
    blocks = lax.all_to_all(cut_along(value, dim, length), axis, 0, 0, tiled=True)
    return jnp.sum(blocks, axis=0)


def sum_by_axis(value, axes, dim):
    far, near = axes
    blocks = cut_along(value, dim, lax.axis_size(far))
    nearer = sent_and_summed(blocks, near, dim + 1)
    arrived = lax.all_to_all(nearer, far, split_axis=0, concat_axis=0, tiled=True)
    return arrived.sum(axis=0)


def nested_sum(value, axes):
    padded = filled_up(value, lax.axis_size(axes[0]) * lax.axis_size(axes[1]))
    whole = gather_axes(sum_by_axis(padded, axes, 0), axes, 0)
    return lax.slice_in_dim(whole, 0, len(value)).reshape(value.shape)


def together(arrays, axis):
    vector, at, outs = (jnp.concatenate([a.reshape(-1) for a in arrays]), 0, [])
    subtotal = nested_sum(vector, axis)
    for a in arrays:
        outs.append(subtotal[at : at + a.size].reshape(a.shape))
        at += a.size
    return tuple(outs)


def side_by_side(arrays, axis, split_dim, concat_dim, along):
    widths = [a.shape[along] for a in arrays]
    both = jnp.concatenate(arrays, axis=along)
    filled = lax.all_to_all(both, axis, split_axis=split_dim, concat_axis=concat_dim, tiled=True)
    return tuple(jnp.split(filled, [sum(widths[:k]) for k in range(1, len(widths))], axis=along))


def gathered_copies(value, axis, dim):
    blocks = copy_for_each(value, axis)
    return laid_out(blocks, dim)


def taken_together(value, axis):
    return copy_for_each(value, axis).astype(jnp.float32).sum(axis=0)


def one_axis_at_a_time(value, axes):
    return functools.reduce(lax.psum, axes, value)


def rotate(component, places):
    half_width = component.shape[-1] // 2
    frequency = rope_base ** (-jnp.arange(half_width, dtype=jnp.float32) / half_width)
    angles = places.astype(jnp.float32)[:, None] * frequency[None, :]
    target_shape = (places.shape[0],) + (1,) * (component.ndim - 2) + (half_width,)
    cosine = jnp.cos(angles).reshape(target_shape)
    sine_part = jnp.sin(angles).reshape(target_shape)
    front_half = component[..., :half_width]
    back_half = component[..., half_width:]
    return jnp.concatenate(
        [front_half * cosine - back_half * sine_part, back_half * cosine + front_half * sine_part],
        axis=-1,
    )


def normalize(values, scales):
    return (
        values
        * lax.rsqrt(jnp.mean(values * values, axis=-1, keepdims=True) + epsilon)
        * scales.astype(jnp.float32)
    )


def ancestry(parents):
    seq_count, prop_count = parents.shape
    slot_ids = jnp.arange(prop_count, dtype=jnp.int32)
    parent_links = (parents[:, :, None] == slot_ids[None, None, :]).astype(jnp.float32)
    identity = jnp.broadcast_to(jnp.eye(prop_count, dtype=jnp.float32), parent_links.shape)
    reached = jnp.minimum(identity + parent_links, 1.0)
    for repeat in range((prop_count - 1).bit_length()):
        reached = jnp.minimum(
            jnp.einsum("sij,sjk->sik", reached, reached, precision=lax.Precision.HIGHEST), 1.0
        )
    depths = (jnp.sum(reached, axis=-1) - 1.0).astype(jnp.int32)
    return (reached, depths)


def down_terms(features, gain_rows, query_down, key_down):
    as_float = features.astype(jnp.float32)
    scaled = (as_float * gain_rows.astype(jnp.float32)).astype(jnp.bfloat16)
    squares = jnp.sum(as_float * as_float, axis=-1)
    query_segment = jnp.dot(scaled, query_down, preferred_element_type=jnp.float32)
    key_segment = jnp.dot(scaled, key_down, preferred_element_type=jnp.float32)
    return (squares, query_segment, key_segment)


def partial_attend(queries, key_rows, slot_index, onehot, reached, kv_rank, value_locally):
    score_scale = (NOPE_DIM + ROPE_DIM) ** (-0.5)
    ancestors = jnp.einsum("sij,snj->sin", reached, onehot, precision=lax.Precision.HIGHEST)
    visible = ((slot_index < 0)[:, None, :] | (ancestors > 0.5))[:, :, None, :]
    scores = (
        jnp.einsum("siha,sna->sihn", queries, key_rows, preferred_element_type=jnp.float32)
        * score_scale
    )
    masked = jnp.where(visible, scores, score_after_mask)
    maxima = jnp.max(masked, axis=-1)
    weights = jnp.where(visible, jnp.exp(masked - maxima[..., None]), 0.0)
    totals = jnp.sum(weights, axis=-1)
    weighted = jnp.einsum(
        "sihn,snk->sihk",
        weights.astype(jnp.bfloat16),
        key_rows[:, :, :kv_rank],
        preferred_element_type=jnp.float32,
    )
    value_fraction = (weighted / jnp.maximum(totals, 1.0)[..., None]).astype(jnp.bfloat16)
    values = jnp.einsum(
        "pwmb,mbe->pwme", value_fraction, value_locally, preferred_element_type=jnp.float32
    )
    return (maxima, totals, values.astype(jnp.bfloat16))


def combine_parts(maxima, totals, values):
    largest = jnp.max(maxima, axis=0)
    shares = totals * jnp.exp(maxima - largest[None])
    summed = jnp.sum(shares[..., None] * values.astype(jnp.float32), axis=0)
    return (summed / jnp.sum(shares, axis=0)[..., None]).astype(jnp.bfloat16)


def local(
    activations,
    latent_cache,
    lengths,
    accepted,
    parents,
    w_query_down,
    w_key_down,
    gain_input,
    gain_query,
    gain_key,
    w_query,
    w_value,
    w_out,
    gain_output,
):
    seq_count, prop_count = parents.shape
    row_count = activations.shape[0]
    heads_here = w_query.shape[1]
    kv_rank = gain_key.shape[0]
    span_len = latent_cache.shape[1]
    reached, depths = ancestry(parents)
    filled = lengths + accepted
    places = (filled[:, None] + depths).reshape(-1)
    squares, query_segment, key_segment = down_terms(
        activations, gain_input, w_query_down, w_key_down
    )
    squares, query_raw, key_raw = together(
        (squares, query_segment, key_segment), (("kv_0", "kv_1", "tp_0"), "tp_1")
    )
    inverse = lax.rsqrt(squares / D + epsilon)[:, None]
    query_low = normalize(query_raw * inverse, gain_query).astype(jnp.bfloat16)
    key_full = key_raw * inverse
    mapped_output = jnp.dot(
        query_low, w_query.reshape(w_query.shape[0], -1), preferred_element_type=jnp.float32
    )
    mapped_output = mapped_output.reshape(row_count, heads_here, -1)
    queries = jnp.concatenate(
        [mapped_output[..., :kv_rank], rotate(mapped_output[..., kv_rank:], places)], axis=-1
    ).astype(jnp.bfloat16)
    fresh_rows = jnp.concatenate(
        [normalize(key_full[:, :kv_rank], gain_key), rotate(key_full[:, kv_rank:], places)], axis=-1
    ).astype(jnp.bfloat16)
    locations_held = lax.axis_index(KV) * span_len + jnp.arange(span_len, dtype=jnp.int32)
    slot_index = locations_held[None, :] - filled[:, None]
    onehot = slot_index[:, :, None] == jnp.arange(prop_count, dtype=jnp.int32)[None, None, :]
    fresh_block = fresh_rows.reshape(seq_count, prop_count, -1)
    placed = jnp.einsum(
        "snj,sja->sna", onehot.astype(jnp.bfloat16), fresh_block, preferred_element_type=jnp.float32
    ).astype(jnp.bfloat16)
    updated = jnp.where(jnp.any(onehot, axis=-1)[:, :, None], placed, latent_cache)
    head_start = lax.axis_index(TP) * heads_here
    value_locally = lax.dynamic_slice_in_dim(w_value, head_start, heads_here, 0)
    maxima, totals, values = partial_attend(
        queries.reshape(seq_count, prop_count, heads_here, -1),
        updated,
        slot_index,
        onehot.astype(jnp.float32),
        reached,
        kv_rank,
        value_locally,
    )
    maxima = maxima.reshape(1, row_count, heads_here)
    totals = totals.reshape(1, row_count, heads_here)
    values = values.reshape(1, row_count, heads_here, -1)
    maxima, totals = side_by_side((maxima, totals), KV, 1, 0, 2)
    values = lax.all_to_all(values, KV, split_axis=1, concat_axis=0, tiled=True)
    combined = combine_parts(maxima, totals, values)
    attended = gathered_copies(combined.reshape(combined.shape[0], -1), KV, 0)
    head_terms = jnp.dot(attended, w_out, preferred_element_type=jnp.float32)
    mixed_raw = taken_together(head_terms.astype(jnp.bfloat16), TP).astype(jnp.float32)
    total_sq = one_axis_at_a_time(jnp.sum(mixed_raw * mixed_raw, axis=-1), KV)
    result = (
        mixed_raw * lax.rsqrt(total_sq / D + epsilon)[:, None] * gain_output.astype(jnp.float32)
    ).astype(jnp.bfloat16)
    return (result, updated)


def solution(mesh):
    split = Mesh(mesh.devices.reshape(4, 4, 4, 2), ("kv_0", "kv_1", "tp_0", "tp_1"))
    return jax.shard_map(
        local,
        mesh=split,
        in_specs=(
            P(None, KV_TP),
            P(None, KV, None),
            P(),
            P(),
            P(),
            P(KV_TP, None),
            P(KV_TP, None),
            P(KV_TP),
            P(),
            P(),
            P(None, TP, None),
            P(),
            P(TP, KV),
            P(KV),
        ),
        out_specs=(P(None, KV), P(None, KV, None)),
        check_vma=False,
    )
```

profile of v0, /device:TPU:0, one launch (start us, length us, event | category | flops | bytes accessed | tf_op | source)
XLA Modules:
  0.0 207.6 jit_solution(10180256169060796957)
XLA Ops:
  2.1 1.1 convolution_bitcast_fusion
  3.4 1.1 fusion.48
  5.0 1.3 reshape_reshape.6
  6.5 4.7 %all_to_all.56 = f32[2,64,2403]{2,1,0:T(8,128)S(1)} all-to-all(f32[2,64,2403]{2,1,0:T(8,128)S(1)} %copy.138), channel_id=1, replica_groups=mesh['kv_0'=4,'kv_1'=4,'tp_0'=4,'tp_1'=2] {'tp_1'}, dimensions={0} | all-to-all | bytes 2460672 | tf_op jit(solution)/shard_map/all_to_all | solution.py:55
  11.3 1.3 all_to_all.39
  12.6 11.5 %all-to-all-start.1 = ((f32[64,1,2403]{2,1,0:T(1,128)}), f32[64,1,2403]{2,1,0:T(1,128)S(1)}, u32[]{:S(2)}, u32[]{:S(2)}) async-start(f32[64,1,2403]{2,1,0:T(1,128)} %all_to_all.39), calls=%async_computation.1 | async-start | bytes 1245184 | tf_op jit(solution)/shard_map/all_to_all | solution.py:63
  26.1 1.1 copy.178
  28.2 10.6 %all-to-all-done.1 = f32[64,1,2403]{2,1,0:T(1,128)S(1)} async-done(((f32[64,1,2403]{2,1,0:T(1,128)}), f32[64,1,2403]{2,1,0:T(1,128)S(1)}, u32[]{:S(2)}, u32[]{:S(2)}) %all-to-all-start.1) | async-done | bytes 615200 | tf_op jit(solution)/shard_map/all_to_all | solution.py:63
  39.1 1.1 broadcast_in_dim.36
  40.3 4.8 %all-to-all-start.2 = ((f32[64,1,2403]{2,1,0:T(1,128)}), f32[64,1,2403]{2,1,0:T(1,128)S(1)}, u32[]{:S(2)}, u32[]{:S(2)}) async-start(f32[64,1,2403]{2,1,0:T(1,128)} %broadcast_in_dim.36), calls=%async_computation.2 | async-start | bytes 1245184 | tf_op jit(solution)/shard_map/all_to_all | solution.py:31
  45.2 2.9 %compare_or_fusion = pred[24,16,2048]{2,1,0:T(8,128)(4,1)} fusion(f32[24,16,16]{2,1,0:T(8,128)S(1)} %get-tuple-element.18, s32[24,2048]{1,0:T(8,128)S(1)} %broadcast_subtract_fusion, pred[24,2048]{1,0:T(8,128)(4,1)S(1)} %broadcast_compare_fusion), kind=kOutput, calls=%fused_computation.18 | convolution fusion | flops 153354240 | bytes 1056768 | tf_op jit(solution)/shard_map/sij,snj->sin/dot_general | solution.py:150
  48.1 10.2 %all-to-all-done.2 = f32[64,1,2403]{2,1,0:T(1,128)S(1)} async-done(((f32[64,1,2403]{2,1,0:T(1,128)}), f32[64,1,2403]{2,1,0:T(1,128)S(1)}, u32[]{:S(2)}, u32[]{:S(2)}) %all-to-all-start.2) | async-done | bytes 615200 | tf_op jit(solution)/shard_map/all_to_all | solution.py:31
  58.4 4.7 %all_to_all.57 = f32[2,64,2403]{2,1,0:T(8,128)S(1)} all-to-all(f32[2,64,2403]{2,1,0:T(8,128)S(1)} %broadcast_in_dim.38), channel_id=1, replica_groups=mesh['kv_0'=4,'kv_1'=4,'tp_0'=4,'tp_1'=2] {'tp_1'}, dimensions={0} | all-to-all | bytes 2460672 | tf_op jit(solution)/shard_map/all_to_all | solution.py:31
  65.1 3.3 %slice.45 = f32[1068,288]{1,0:T(8,128)} reshape(f32[64,2,2403]{2,1,0:T(2,128)S(1)} %copy.139) | data formatting | bytes 2460672 | tf_op jit(solution)/shard_map/slice | solution.py:77
  69.4 1.2 slice.56
  71.6 1.0 broadcast_multiply_fusion
  75.3 2.1 %reshape.265 = f32[384,512]{1,0:T(8,128)} reshape(f32[196608]{0:T(1024)} %slice.51) | data formatting | bytes 1572864 | tf_op jit(solution)/shard_map/reshape | solution.py:77
  77.4 1.4 broadcast_bitcast_fusion.2
  81.4 25.2 %convert_select_fusion = bf16[24,2048,288]{1,2,0:T(8,128)(2,1)} fusion(bf16[24,2048,288]{1,2,0:T(8,128)(2,1)} %param.15, pred[24,2048]{1,0:T(8,128)(4,1)S(1)} %fusion.11, s32[24,2048]{1,0:T(8,128)S(1)} %broadcast_subtract_fusion, bf16[24,16,16]{2,1,0:T(8,128)(2,1)} %bitcast.94, bf16[24,16,16]{2,1,0:T(8,128)(2,1)} %bitcast.93, ...), kind=kOutput, calls=%fused_computation.2 | convolution fusion | flops 482746368 | bytes 57090048 | tf_op jit(solution)/shard_map/snj,sja->sna/dot_general | solution.py:227
  106.6 12.1 %fusion.3 = (f32[24,16,2]{1,2,0:T(2,128)S(1)}, f32[24,16,2,2048]{3,1,2,0:T(8,128)S(1)}) fusion(pred[24,16,2048]{2,1,0:T(8,128)(4,1)S(1)} %copy-done.3, bf16[24,2048,288]{1,2,0:T(8,128)(2,1)} %convert_select_fusion, bf16[24,16,2,16]{3,1,2,0:T(8,128)(2,1)S(1)} %copy.143, bf16[24,16,2,16]{3,1,2,0:T(8,128)(2,1)S(1)} %copy.142, ...), kind=kOutput, calls=%fused_computation.7 | convolution fusion | flops 912014592 | bytes 35834880 | tf_op jit(solution)/shard_map/siha,sna->sihn/dot_general | solution.py:153
  118.8 2.6 %copy-done.2 = f32[24,16,2,2048]{3,1,2,0:T(8,128)} copy-done((f32[24,16,2,2048]{3,1,2,0:T(8,128)}, f32[24,16,2,2048]{3,1,2,0:T(8,128)S(1)}, u32[]{:S(2)}) %copy-start.2) | copy-done | bytes 6291480
  121.4 2.0 fusion.5
  124.5 3.5 %all-to-all-start.4 = ((f32[1,384,4]{2,0,1:T(1,128)}), f32[1,384,4]{2,0,1:T(1,128)S(1)}, u32[]{:S(2)}, u32[]{:S(2)}) async-start(f32[1,384,4]{2,0,1:T(1,128)} %copy.151), calls=%async_computation.4 | async-start | bytes 393216 | tf_op jit(solution)/shard_map/all_to_all | solution.py:85
  128.0 14.2 %fusion.20 = bf16[24,16,2,256]{3,1,2,0:T(8,128)(2,1)S(1)} fusion(bf16[24,2048,288]{1,2,0:T(8,128)(2,1)} %convert_select_fusion, f32[24,16,2,2048]{3,1,2,0:T(8,128)} %copy-done.2, f32[24,16,2]{1,2,0:T(2,128)S(1)} %get-tuple-element.19, pred[24,16,2048]{2,1,0:T(8,128)(4,1)S(1)} %copy-done.3, f32[24,16,2]{1,2,0:T(2,128)S(1)} %broadcast_maximum_fusion), kind=kOutput, calls=%fused_computation.32 | convolution fusion | flops 813563904 | bytes 32643072 | tf_op jit(solution)/shard_map/sihn,snk->sihk/dot_general | solution.py:160
  142.2 1.3 fusion.16
  144.5 7.2 %all-to-all-start.5 = ((bf16[16,2,1536]{2,1,0:T(2,128)(2,1)}), bf16[16,2,1536]{2,1,0:T(2,128)(2,1)S(1)}, u32[]{:S(2)}, u32[]{:S(2)}) async-start(bf16[16,2,1536]{2,1,0:T(2,128)(2,1)} %reshape.277), calls=%async_computation.5 | async-start | bytes 196608 | tf_op jit(solution)/shard_map/all_to_all | solution.py:246
  152.3 7.2 %all-to-all-done.5 = bf16[16,2,1536]{2,1,0:T(2,128)(2,1)S(1)} async-done(((bf16[16,2,1536]{2,1,0:T(2,128)(2,1)}), bf16[16,2,1536]{2,1,0:T(2,128)(2,1)S(1)}, u32[]{:S(2)}, u32[]{:S(2)}) %all-to-all-start.5) | async-done | bytes 98336 | tf_op jit(solution)/shard_map/all_to_all | solution.py:246
  160.2 10.9 %all_to_all.58 = bf16[16,24,128]{2,1,0:T(8,128)(2,1)S(1)} all-to-all(bf16[16,24,128]{2,1,0:T(8,128)(2,1)S(1)} %broadcast_in_dim.46), channel_id=1, replica_groups=mesh['kv_0'=4,'kv_1'=4,'tp_0'=4,'tp_1'=2] {'kv_0','kv_1'}, dimensions={0} | all-to-all | bytes 196608 | tf_op jit(solution)/shard_map/all_to_all | solution.py:31
  172.3 3.5 %all-to-all-start.7 = ((bf16[8,384,128]{2,1,0:T(8,128)(2,1)}), bf16[8,384,128]{2,1,0:T(8,128)(2,1)S(1)}, u32[]{:S(2)}, u32[]{:S(2)}) async-start(bf16[8,384,128]{2,1,0:T(8,128)(2,1)} %broadcast_in_dim.47), calls=%async_computation.7 | async-start | bytes 1572864 | tf_op jit(solution)/shard_map/all_to_all | solution.py:31
  175.9 13.0 %all-to-all-done.7 = bf16[8,384,128]{2,1,0:T(8,128)(2,1)S(1)} async-done(((bf16[8,384,128]{2,1,0:T(8,128)(2,1)}), bf16[8,384,128]{2,1,0:T(8,128)(2,1)S(1)}, u32[]{:S(2)}, u32[]{:S(2)}) %all-to-all-start.7) | async-done | bytes 786464 | tf_op jit(solution)/shard_map/all_to_all | solution.py:31
  189.1 8.7 %psum.14 = f32[384]{0:T(512)S(1)} all-reduce(f32[384]{0:T(512)S(1)} %multiply_reduce_fusion.2), channel_id=1, replica_groups=mesh['kv_0'=4,'kv_1'=4,'tp_0'=4,'tp_1'=2] {'kv_0'}, use_global_device_ids=true, to_apply=%region_14.15 | all-reduce | flops 384 | bytes 3072 | tf_op jit(solution)/shard_map/psum | solution.py:99
  197.9 8.9 %psum.15 = f32[384]{0:T(512)S(1)} all-reduce(f32[384]{0:T(512)S(1)} %psum.14), channel_id=1, replica_groups=mesh['kv_0'=4,'kv_1'=4,'tp_0'=4,'tp_1'=2] {'kv_1'}, use_global_device_ids=true, to_apply=%region_15.16 | all-reduce | flops 384 | bytes 3072 | tf_op jit(solution)/shard_map/psum | solution.py:99
  (108 shorter events, 20.4 us)
Async XLA Ops:
  0.6 79.2 %copy-start = (bf16[512,2,288]{0,2,1:T(8,128)(2,1)S(1)}, bf16[512,2,288]{0,2,1:T(8,128)(2,1)}, u32[]{:S(2)}) copy-start(bf16[512,2,288]{0,2,1:T(8,128)(2,1)} %param.24) | copy-start | bytes 1769476
  5.0 19.2 %copy-start.9 = (bf16[256]{0:T(256)(128)(2,1)S(1)}, bf16[256]{0:T(256)(128)(2,1)}, u32[]{:S(2)}) copy-start(bf16[256]{0:T(256)(128)(2,1)} %param.23) | copy-start | bytes 1540
  5.0 19.2 %copy-start.7 = (s32[24,16]{0,1:T(8,128)S(1)}, s32[24,16]{0,1:T(8,128)}, u32[]{:S(2)}) copy-start(s32[24,16]{0,1:T(8,128)} %param.18) | copy-start | bytes 4612
  6.3 19.4 %copy-start.10 = (s32[24]{0:T(128)S(1)}, s32[24]{0:T(128)}, u32[]{:S(2)}) copy-start(s32[24]{0:T(128)} %param.16) | copy-start | bytes 292
  6.4 19.4 %copy-start.11 = (s32[24]{0:T(128)S(1)}, s32[24]{0:T(128)}, u32[]{:S(2)}) copy-start(s32[24]{0:T(128)} %param.17) | copy-start | bytes 292
  6.4 19.6 %copy-start.8 = (bf16[512]{0:T(512)(128)(2,1)S(1)}, bf16[512]{0:T(512)(128)(2,1)}, u32[]{:S(2)}) copy-start(bf16[512]{0:T(512)(128)(2,1)} %param.22) | copy-start | bytes 3076
  12.6 26.1 %all-to-all-start.1 = ((f32[64,1,2403]{2,1,0:T(1,128)}), f32[64,1,2403]{2,1,0:T(1,128)S(1)}, u32[]{:S(2)}, u32[]{:S(2)}) async-start(f32[64,1,2403]{2,1,0:T(1,128)} %all_to_all.39), calls=%async_computation.1 | async-start | bytes 1245184 | tf_op jit(solution)/shard_map/all_to_all | solution.py:63
  40.3 18.0 %all-to-all-start.2 = ((f32[64,1,2403]{2,1,0:T(1,128)}), f32[64,1,2403]{2,1,0:T(1,128)S(1)}, u32[]{:S(2)}, u32[]{:S(2)}) async-start(f32[64,1,2403]{2,1,0:T(1,128)} %broadcast_in_dim.36), calls=%async_computation.2 | async-start | bytes 1245184 | tf_op jit(solution)/shard_map/all_to_all | solution.py:31
  69.4 10.0 %copy-start.4 = (f32[48,4,8,128]{3,1,2,0:T(4,128)S(1)}, f32[48,4,8,128]{3,1,2,0:T(4,128)}, u32[]{:S(2)}) copy-start(f32[48,4,8,128]{3,1,2,0:T(4,128)} %copy.178) | copy-start | bytes 2359300
  78.9 2.5 %copy-start.5 = (bf16[384,256]{1,0:T(8,128)(2,1)S(1)}, bf16[384,256]{1,0:T(8,128)(2,1)}, u32[]{:S(2)}) copy-start(bf16[384,256]{1,0:T(8,128)(2,1)} %copy.146) | copy-start | bytes 589828
  81.4 25.2 %copy-start.3 = (pred[24,16,2048]{2,1,0:T(8,128)(4,1)S(1)}, pred[24,16,2048]{2,1,0:T(8,128)(4,1)}, u32[]{:S(2)}) copy-start(pred[24,16,2048]{2,1,0:T(8,128)(4,1)} %compare_or_fusion) | copy-start | bytes 2359300
  118.7 2.7 %copy-start.2 = (f32[24,16,2,2048]{3,1,2,0:T(8,128)}, f32[24,16,2,2048]{3,1,2,0:T(8,128)S(1)}, u32[]{:S(2)}) copy-start(f32[24,16,2,2048]{3,1,2,0:T(8,128)S(1)} %get-tuple-element.20) | copy-start | bytes 18874372
  124.5 20.1 %all-to-all-start.4 = ((f32[1,384,4]{2,0,1:T(1,128)}), f32[1,384,4]{2,0,1:T(1,128)S(1)}, u32[]{:S(2)}, u32[]{:S(2)}) async-start(f32[1,384,4]{2,0,1:T(1,128)} %copy.151), calls=%async_computation.4 | async-start | bytes 393216 | tf_op jit(solution)/shard_map/all_to_all | solution.py:85
  128.0 43.2 %copy-start.6 = (bf16[128,128]{1,0:T(8,128)(2,1)S(1)}, bf16[128,128]{1,0:T(8,128)(2,1)}, u32[]{:S(2)}) copy-start(bf16[128,128]{1,0:T(8,128)(2,1)} %param.26) | copy-start | bytes 98308
  128.0 79.6 %copy-start.1 = (bf16[512,2,288]{0,2,1:T(8,128)(2,1)S(1)}, bf16[512,2,288]{0,2,1:T(8,128)(2,1)}, u32[]{:S(2)}) copy-start(bf16[512,2,288]{0,2,1:T(8,128)(2,1)} %param.24) | copy-start | bytes 1769476
  142.2 33.7 %copy-start.12 = (bf16[128]{0:T(256)(128)(2,1)S(1)}, bf16[128]{0:T(256)(128)(2,1)}, u32[]{:S(2)}) copy-start(bf16[128]{0:T(256)(128)(2,1)} %param.27) | copy-start | bytes 772
  144.5 15.0 %all-to-all-start.5 = ((bf16[16,2,1536]{2,1,0:T(2,128)(2,1)}), bf16[16,2,1536]{2,1,0:T(2,128)(2,1)S(1)}, u32[]{:S(2)}, u32[]{:S(2)}) async-start(bf16[16,2,1536]{2,1,0:T(2,128)(2,1)} %reshape.277), calls=%async_computation.5 | async-start | bytes 196608 | tf_op jit(solution)/shard_map/all_to_all | solution.py:246
  172.3 16.6 %all-to-all-start.7 = ((bf16[8,384,128]{2,1,0:T(8,128)(2,1)}), bf16[8,384,128]{2,1,0:T(8,128)(2,1)S(1)}, u32[]{:S(2)}, u32[]{:S(2)}) async-start(bf16[8,384,128]{2,1,0:T(8,128)(2,1)} %broadcast_in_dim.47), calls=%async_computation.7 | async-start | bytes 1572864 | tf_op jit(solution)/shard_map/all_to_all | solution.py:31
where the time goes:
time: 209 us; the launch traced here: 208 us
  matrix products  59.9 us (29%)
  waiting for transfers between devices  41 us (20%)
  blocking collectives  38.1 us (18%)
  starting transfers between devices  30.5 us (15%)
  local copies, waits for them, and re-layouts  27 us (13%)
  other arithmetic  9.9 us (5%)
    dot_general x1, matrix products, local(): jnp.einsum('snj,sja->sna', onehot.astype(jnp.bfloat16), fresh_block, pref...  25.2 us
    all_to_all x2, waiting for transfers between devices, copy_for_each(): lax.all_to_all(jnp.broadcast_to(value[None], (length, *value.shape)), axi...  23.2 us
    psum x2, blocking collectives, one_axis_at_a_time(): return functools.reduce(lax.psum, axes, value)  17.7 us
    all_to_all x2, blocking collectives, copy_for_each(): lax.all_to_all(jnp.broadcast_to(value[None], (length, *value.shape)), axi...  15.7 us
    dot_general x1, matrix products, partial_attend(): jnp.einsum('sihn,snk->sihk', weights.astype(jnp.bfloat16), key_rows[:, :,...  14.2 us
    dot_general x1, matrix products, partial_attend(): jnp.einsum('siha,sna->sihn', queries, key_rows, preferred_element_type=jn...  12.1 us
    all_to_all x1, starting transfers between devices, sum_by_axis(): lax.all_to_all(nearer, far, split_axis=0, concat_axis=0, tiled=True)  11.5 us
    all_to_all x1, waiting for transfers between devices, sum_by_axis(): lax.all_to_all(nearer, far, split_axis=0, concat_axis=0, tiled=True)  10.6 us
  transfers between devices with their start and end apart: 5, of which 4 were waited for; matrix products, arithmetic and copies ran while one was open for 12% of the time, Pallas kernels for 0%

commit v1 on v0

v1 whole, which is shorter than its diff:
```python
import jax
import jax.numpy as jnp
from jax import lax
from jax.experimental import pallas as pl
from jax.experimental.pallas import tpu as pltpu
from jax.sharding import PartitionSpec as P


f32 = jnp.float32
bf16 = jnp.bfloat16

D = 2048
SEQS = 24
PROPS = 16
SPAN = 2048
ROPE_DIM = 32
LINES = 288
SCALE = 96.0 ** (-0.5)
EPS = 1e-06
ROPE_BASE = 10000.0
MASKED = -1e30
ALL = ("kv", "tp")
VMEM = pltpu.VMEM


def vmem_spec():
    return pl.BlockSpec(memory_space=pltpu.VMEM)


def smem_spec():
    return pl.BlockSpec(memory_space=pltpu.SMEM)


def any_spec():
    return pl.BlockSpec(memory_space=pl.ANY)


def cost(flops, moved):
    return pl.CostEstimate(flops=int(flops), bytes_accessed=int(moved), transcendentals=0)


def call(kernel, out_shape, inputs, price, scratch=(), limit=16):
    many = isinstance(out_shape, tuple)
    return pl.pallas_call(
        kernel,
        out_shape=out_shape,
        in_specs=[vmem_spec()] * inputs,
        out_specs=(vmem_spec(),) * len(out_shape) if many else vmem_spec(),
        scratch_shapes=list(scratch),
        cost_estimate=price,
        compiler_params=pltpu.CompilerParams(vmem_limit_bytes=limit << 20),
    )


def dot_nt(a, b):
    return lax.dot_general(a, b, (((1,), (1,)), ((), ())), preferred_element_type=f32)


def dot_nn(a, b):
    return lax.dot_general(a, b, (((1,), (0,)), ((), ())), preferred_element_type=f32)


def dot_tn(a, b):
    return lax.dot_general(a, b, (((0,), (0,)), ((), ())), preferred_element_type=f32)


def turn(v, n):
    return pltpu.roll(v, n % 128, v.ndim - 1)


def lanes_of(shape):
    return lax.broadcasted_iota(jnp.int32, shape, len(shape) - 1)


def rounded(v):
    return v.astype(bf16).astype(f32)


def pack_kernel(a_ref, q_ref, k_ref, g_ref, o_ref):
    row = lax.broadcasted_iota(jnp.int32, (384, 512), 0)
    place = (row & 15) * 32 + (row >> 4)
    pick = jnp.where(lanes_of((384, 512)) == place, 1.0, 0.0).astype(bf16)
    lines = dot_nn(a_ref[...], pick)
    lane = lanes_of((16, 128))
    gain = jnp.broadcast_to(g_ref[...], (16, 16))
    diagonal = lax.broadcasted_iota(jnp.int32, (16, 16), 0) == lanes_of((16, 16))
    gain = jnp.sum(jnp.where(diagonal, gain, 0.0), axis=1, keepdims=True)
    query = q_ref[...].astype(f32)
    key = k_ref[...].astype(f32)
    rope = jnp.concatenate([key[:, 256:288], jnp.zeros((16, 96), f32)], axis=1)
    columns = []
    for t in range(8):
        tile = query[:, (t // 2) * 128 : (t // 2) * 128 + 128]
        line = turn(tile, 24 - (t % 2) * 64)
        tile = key[:, (t // 4) * 128 : (t // 4) * 128 + 128]
        line = jnp.where(lane < 88, line, turn(tile, 88 - (t % 4) * 32))
        line = jnp.where(lane < 120, line, turn(rope, 120 - 4 * t))
        columns.append(jnp.where(lane < 124, line, jnp.where(lane == 124, gain, 0.0)))
    for j in range(16):
        tile = lines[:, (j // 4) * 128 : (j // 4) * 128 + 128]
        tile = turn(tile, -(j % 4) * 32) if j % 4 else tile
        for t in range(8):
            o_ref[j * 8 + t] = jnp.where(lane < 24, tile, columns[t]).astype(bf16)


def pack(a, q, k, g):
    return call(
        pack_kernel, jax.ShapeDtypeStruct((128, 16, 128), bf16), 4, cost(1e8, 1e6)
    )(a, q, k, g)


def down_kernel(x_ref, o_ref):
    x = x_ref[...]
    wide = x.astype(f32)
    lane = lanes_of(wide.shape)
    scaled = wide * wide[:, 124:125]
    lhs = jnp.where(lane < 24, scaled, turn(wide, 32)).astype(bf16)
    out = dot_tn(lhs, x)
    cross = out[32:56, :]
    row = lax.broadcasted_iota(jnp.int32, cross.shape, 0)
    squares = jnp.sum(jnp.where(row == lanes_of(cross.shape), cross, 0.0), axis=1, keepdims=True)
    o_ref[...] = jnp.broadcast_to(out[0:24, :] * lax.rsqrt(squares / D + EPS), o_ref.shape)


def down(x):
    return call(
        down_kernel,
        jax.ShapeDtypeStruct((8, 24, 128), f32),
        1,
        cost(2 * 128 * 128 * 2048, x.size * 2),
    )(x)


def query_kernel(t_ref, y_ref, gq_ref, gk_ref, cos_ref, sin_ref, w_ref, o_ref, block):
    mine = t_ref[0]
    lane = lanes_of((24, 128))
    parts = [y_ref[t] for t in range(8)]
    raw = [
        jnp.where(lane < 64, turn(parts[2 * a], -24), turn(parts[2 * a + 1], 40)) for a in range(4)
    ]
    squares = sum(jnp.sum(r * r, axis=1, keepdims=True) for r in raw)
    scale = lax.rsqrt(squares / 512.0 + EPS)
    low = jnp.concatenate(
        [raw[a] * scale * gq_ref[a : a + 1, :] for a in range(4)], axis=1
    ).astype(bf16)
    lats = []
    for half in range(2):
        lat = turn(parts[4 * half], -88)
        for u in range(1, 4):
            lat = jnp.where(lane >= u * 32, turn(parts[4 * half + u], u * 32 - 88), lat)
        lats.append(lat)
    squares = sum(jnp.sum(r * r, axis=1, keepdims=True) for r in lats)
    scale = lax.rsqrt(squares / 256.0 + EPS)
    lats = [rounded(lats[h] * scale * gk_ref[h : h + 1, :]) for h in range(2)]
    turned = turn(parts[0], -120)
    for t in range(1, 8):
        turned = jnp.where(lane >= 4 * t, turn(parts[t], 4 * t - 120), turned)
    cosine, sine = cos_ref[...], sin_ref[...]

    def rotate(v):
        partner = jnp.where(lane < 16, turn(v, -16), turn(v, 16))
        return v * cosine + partner * sine

    def own(tile):
        row = lax.broadcasted_iota(jnp.int32, tile.shape, 0)
        line = jnp.sum(jnp.where(row == mine, tile, 0.0), axis=0, keepdims=True)
        return jnp.broadcast_to(line, tile.shape)

    key_rope = rounded(rotate(turned))
    ropes = []
    query_rope = []
    for hh in range(2):
        lat = dot_nt(low, w_ref[hh, 0:256, :])
        rope = dot_nt(low, w_ref[hh, 256:288, :])
        rope = rotate(jnp.concatenate([rope, jnp.zeros((24, 96), f32)], axis=1))
        query_rope.append(rope)
        for s in range(3):
            for half in range(2):
                block[:, (s * 2 + hh) * 2 + half, :] = lat[
                    s * 8 : s * 8 + 8, half * 128 : half * 128 + 128
                ]
    for s in range(3):
        for half in range(2):
            block[:, 12 + s * 2 + half, :] = own(lats[half][s * 8 : s * 8 + 8, :])
    for s in range(3):
        for hh in range(2):
            ropes.append(query_rope[hh][s * 8 : s * 8 + 8, :])
    for s in range(3):
        ropes.append(own(key_rope[s * 8 : s * 8 + 8, :]))
    small = lanes_of((8, 128))
    for row in range(3):
        line = jnp.zeros((8, 128), f32)
        for n in range(4 * row, min(4 * row + 4, 9)):
            at = (n % 4) * 32
            line = jnp.where((small >= at) & (small < at + 32), turn(ropes[n], at), line)
        block[:, 18 + row, :] = line
        block[:, 21 + row, :] = jnp.zeros((8, 128), f32)
    packed = block[...].astype(bf16)
    for copy in range(16):
        o_ref[copy * 8 : copy * 8 + 8] = packed


def queries(mine, y, gq, gk, cosine, sine, w):
    return pl.pallas_call(
        query_kernel,
        out_shape=jax.ShapeDtypeStruct((128, 24, 128), bf16),
        in_specs=[smem_spec()] + [vmem_spec()] * 6,
        out_specs=vmem_spec(),
        scratch_shapes=[VMEM((8, 24, 128), f32)],
        cost_estimate=cost(2 * 24 * 512 * 576, 128 * 24 * 256),
        compiler_params=pltpu.CompilerParams(vmem_limit_bytes=16 << 20),
        name="queries",
    )(mine, y, gq, gk, cosine, sine, w)


CHUNK = 512


def attend_kernel(
    n_ref, z_ref, cache_ref, anc_ref, wv_ref, o_ref, fresh_ref, keys, wide, lines, part, lam, score, sems
):
    mine = n_ref[24]

    def fetch(s):
        return pltpu.make_async_copy(cache_ref.at[s * 8 + mine], keys.at[s], sems.at[s])

    for s in range(3):
        fetch(s).start()
    wide[...] = z_ref[...].astype(f32)
    lane = lanes_of((128, 128))
    packed = [wide[:, 18 + r, :] for r in range(3)]

    def rope_of(n):
        v = packed[n // 4]
        v = turn(v, -(n % 4) * 32) if n % 4 else v
        return jnp.where(lane < 32, v, 0.0)

    for s in range(3):
        for half in range(2):
            lines[s, half] = wide[:, 12 + s * 2 + half, :]
        lines[s, 2] = rope_of(6 + s)

    def fresh_of(s, t):
        return jnp.concatenate(
            [lines[s, a, pl.ds(t, 16, stride=8), :] for a in range(3)], axis=1
        ).astype(bf16)

    for s in range(3):
        for t in range(8):
            fresh_ref[s * 8 + t] = fresh_of(s, t)
    slot = lanes_of((256, 16))
    for s in range(3):
        off = n_ref[s * 8 + mine]
        fresh = fresh_of(s, mine)
        lat = jnp.concatenate(
            [
                jnp.concatenate(
                    [wide[:, (s * 2 + hh) * 2, :], wide[:, (s * 2 + hh) * 2 + 1, :]], axis=1
                )
                for hh in range(2)
            ],
            axis=0,
        ).astype(bf16)
        rope = jnp.concatenate([rope_of(s * 2 + hh)[:, 0:32] for hh in range(2)], axis=0).astype(
            bf16
        )
        near = (dot_nt(lat, fresh[:, 0:256]) + dot_nt(rope, fresh[:, 256:288])) * SCALE
        anc = anc_ref[s][:, 0:16]
        seen = (
            (jnp.concatenate([anc, anc], axis=0) > 0.5) & (slot + off >= 0) & (slot + off < SPAN)
        )
        near = jnp.where(seen, near, MASKED)
        top = jnp.max(near, axis=1, keepdims=True)
        fetch(s).wait()
        for c in range(SPAN // CHUNK):
            cols = slice(c * CHUNK, (c + 1) * CHUNK)
            got = (
                dot_nn(lat, keys[s, 0:256, cols]) + dot_nn(rope, keys[s, 256:288, cols])
            ) * SCALE
            got = jnp.where(lanes_of(got.shape) + c * CHUNK < off, got, MASKED)
            score[:, cols] = got
            top = jnp.maximum(top, jnp.max(got, axis=1, keepdims=True))
        weight = jnp.where(seen, jnp.exp(near - top), 0.0)
        total = jnp.sum(weight, axis=1, keepdims=True)
        acc = dot_nn(weight.astype(bf16), fresh[:, 0:256])
        for c in range(SPAN // CHUNK):
            cols = slice(c * CHUNK, (c + 1) * CHUNK)
            got = score[:, cols]
            weight = jnp.where(
                lanes_of(got.shape) + c * CHUNK < off, jnp.exp(got - top), 0.0
            )
            total = total + jnp.sum(weight, axis=1, keepdims=True)
            acc = acc + dot_nt(weight.astype(bf16), keys[s, 0:256, cols])
        acc = rounded(acc / jnp.maximum(total, 1.0))
        for half in range(2):
            part[s, half] = acc[:, half * 128 : half * 128 + 128]
        level = jnp.where(total > 0.0, top + jnp.log(jnp.maximum(total, 1.0)), MASKED)
        lam[s] = jnp.broadcast_to(level, (256, 128))
    small = lanes_of((8, 128))
    for h in range(16):
        pieces = []
        level = jnp.zeros((8, 128), f32)
        for half in range(2):
            for s in range(3):
                rows = pl.ds((h % 2) * 128 + half * 64 + h // 2, 8, stride=8)
                pieces.append(jnp.concatenate([part[s, a, rows, :] for a in range(2)], axis=1))
                level = jnp.where(small // 4 == half * 3 + s, lam[s, rows, :], level)
        out = dot_nt(jnp.concatenate(pieces, axis=0).astype(bf16), wv_ref[h])
        out = jnp.concatenate([out[0:24], out[24:48]], axis=1)
        first = rounded(level)
        second = rounded(level - first)
        third = (level - first) - second
        level = jnp.where(small % 4 == 0, first, jnp.where(small % 4 == 1, second, third))
        level = jnp.where(small % 4 == 3, 0.0, level)
        o_ref[h] = jnp.concatenate([out, level], axis=0).astype(bf16)


def attend(numbers, z, cache, anc, wv):
    return pl.pallas_call(
        attend_kernel,
        out_shape=(
            jax.ShapeDtypeStruct((16, 32, 128), bf16),
            jax.ShapeDtypeStruct((24, 16, 384), bf16),
        ),
        in_specs=[smem_spec(), vmem_spec(), any_spec(), vmem_spec(), vmem_spec()],
        out_specs=(vmem_spec(), vmem_spec()),
        scratch_shapes=[
            VMEM((3, LINES, SPAN), bf16),
            VMEM((128, 24, 128), f32),
            VMEM((3, 3, 128, 128), f32),
            VMEM((3, 2, 256, 128), f32),
            VMEM((3, 256, 128), f32),
            VMEM((256, SPAN), f32),
            pltpu.SemaphoreType.DMA((3,)),
        ],
        cost_estimate=cost(3 * 2 * 256 * 2048 * 544, 3 * LINES * SPAN * 2),
        compiler_params=pltpu.CompilerParams(vmem_limit_bytes=40 << 20),
        name="attend",
    )(numbers, z, cache, anc, wv)


def combine_kernel(v_ref, o_ref):
    v = v_ref[...].astype(f32)
    level = v[:, 24:32, :]
    level = (level + turn(level, -1)) + turn(level, -2)
    lane = lanes_of((16, 8, 128))
    outs = []
    for s in range(3):
        low, high = (level[:, :, 4 * (h * 3 + s) : 4 * (h * 3 + s) + 1] for h in range(2))
        both = jnp.where(lane < 64, low, high)
        share = jnp.exp(both - jnp.max(both, axis=0, keepdims=True))
        summed = jnp.sum(share * v[:, s * 8 : s * 8 + 8, :], axis=0)
        outs.append(summed / jnp.sum(share, axis=0))
    o_ref[...] = jnp.broadcast_to(jnp.concatenate(outs, axis=0).astype(bf16), o_ref.shape)


def combine(v):
    return call(combine_kernel, jax.ShapeDtypeStruct((16, 24, 128), bf16), 1, cost(1e6, 1e5))(v)


def mix_kernel(t_ref, u_ref, *refs):
    w_refs, (o_ref, s_ref) = refs[:8], refs[8:]
    lane = lanes_of((24, 128))
    mixed = jnp.zeros((48, 128), f32)
    for k in range(8):
        p = (t_ref[0] - k) & 7
        a, b = u_ref[2 * p].astype(f32), u_ref[2 * p + 1].astype(f32)
        left = jnp.where(lane < 64, a, turn(b, 64))
        right = jnp.where(lane < 64, turn(a, 64), b)
        lhs = jnp.concatenate([left, right], axis=0).astype(bf16)
        mixed = mixed + dot_nn(lhs, w_refs[k][...])
    o_ref[...] = mixed
    squares = jnp.broadcast_to(jnp.sum(mixed * mixed, axis=1, keepdims=True), mixed.shape)
    row = lax.broadcasted_iota(jnp.int32, (48, 128), 0)
    line = jnp.sum(jnp.where(row == lanes_of((48, 128)), squares, 0.0), axis=0, keepdims=True)
    s_ref[...] = jnp.broadcast_to(line[None], s_ref.shape)


def mix(t, u, w):
    return pl.pallas_call(
        mix_kernel,
        out_shape=(
            jax.ShapeDtypeStruct((48, 128), f32),
            jax.ShapeDtypeStruct((16, 8, 128), f32),
        ),
        in_specs=[smem_spec()] + [vmem_spec()] * 9,
        out_specs=(vmem_spec(),) * 2,
        cost_estimate=cost(2 * 48 * 1024 * 128, 4e5),
        compiler_params=pltpu.CompilerParams(vmem_limit_bytes=16 << 20),
        name="mix",
    )(t, u, *w)


def finish_kernel(m_ref, s_ref, g_ref, o_ref):
    total = jnp.sum(s_ref[...], axis=0)[0:1]
    inverse = lax.rsqrt(total / D + EPS)
    row = lax.broadcasted_iota(jnp.int32, (48, 128), 0)
    same = row == lanes_of((48, 128))
    column = jnp.sum(jnp.where(same, inverse, 0.0), axis=1, keepdims=True)
    out = m_ref[...] * column * g_ref[...]
    rows = []
    for s in range(3):
        rows += [out[s * 8 : s * 8 + 8], out[24 + s * 8 : 32 + s * 8]]
    rows = jnp.concatenate(rows, axis=0).astype(bf16)
    o_ref[...] = jnp.broadcast_to(rows, o_ref.shape)


def finish(m, s, g):
    return call(finish_kernel, jax.ShapeDtypeStruct((8, 48, 128), bf16), 3, cost(1e6, 4e5))(m, s, g)


def spread_kernel(m_ref, o_ref):
    for t in range(8):
        for s in range(3):
            o_ref[(s * 8 + t) * 16 : (s * 8 + t) * 16 + 16, :] = m_ref[t, s * 16 : s * 16 + 16]


def spread(m):
    return call(spread_kernel, jax.ShapeDtypeStruct((384, 128), bf16), 1, cost(1e6, 4e5))(m)


DEPTH = 4


def copy_rows(source, target, buffer, into, outof, start, stop):
    count = stop - start

    def read(n, b):
        return pltpu.make_async_copy(source.at[start + n], buffer.at[b], into.at[b])

    def write(n, b):
        return pltpu.make_async_copy(buffer.at[b], target.at[start + n], outof.at[b])

    for n in range(min(DEPTH, count)):
        read(n, n).start()

    def body(n, carry):
        b = lax.rem(n, 2 * DEPTH)
        read(n, b).wait()
        write(n, b).start()

        @pl.when(n + DEPTH < count)
        def _():
            later = lax.rem(n + DEPTH, 2 * DEPTH)

            @pl.when(n >= DEPTH)
            def _():
                write(n - DEPTH, later).wait()

            read(n + DEPTH, later).start()

        return carry

    lax.fori_loop(0, count, body, 0)

    def drain(n, carry):
        write(n, lax.rem(n, 2 * DEPTH)).wait()
        return carry

    lax.fori_loop(max(0, count - 2 * DEPTH), count, drain, 0)


def copy_cache(cache, so_far, start, stop):
    def kernel(*refs):
        source = refs[0]
        target, buffer, into, outof = refs[-4:]
        copy_rows(source, target, buffer, into, outof, start, stop)

    first = so_far is None
    return pl.pallas_call(
        kernel,
        out_shape=jax.ShapeDtypeStruct(cache.shape, cache.dtype),
        in_specs=[any_spec()] * (1 if first else 2),
        out_specs=any_spec(),
        scratch_shapes=[
            VMEM((2 * DEPTH, LINES, SPAN), bf16),
            pltpu.SemaphoreType.DMA((2 * DEPTH,)),
            pltpu.SemaphoreType.DMA((2 * DEPTH,)),
        ],
        input_output_aliases={} if first else {1: 0},
        cost_estimate=cost((stop - start) * 9e8, (stop - start) * LINES * SPAN * 4),
        compiler_params=pltpu.CompilerParams(vmem_limit_bytes=40 << 20),
        name="copy_cache",
    )(*((cache,) if first else (cache, so_far)))


WINDOW = 256


def place_kernel(n_ref, cache_ref, fresh_ref, old_ref, o_ref, buffer, into, outof):
    def where_is(s):
        off = n_ref[s]
        hit = (off > -PROPS) & (off < SPAN)
        first = jnp.clip(off, 0, SPAN - 1)
        first = jnp.minimum((first // 128) * 128, SPAN - WINDOW)
        return off, hit, pl.multiple_of(first, 128)

    def read(s, first):
        return pltpu.make_async_copy(
            cache_ref.at[s, :, pl.ds(first, WINDOW)], buffer.at[s], into.at[s]
        )

    def write(s, first):
        return pltpu.make_async_copy(
            buffer.at[s], o_ref.at[s, :, pl.ds(first, WINDOW)], outof.at[s]
        )

    def begin(s, carry):
        _, hit, first = where_is(s)

        @pl.when(hit)
        def _():
            read(s, first).start()

        return carry

    def change(s, carry):
        off, hit, first = where_is(s)

        @pl.when(hit)
        def _():
            read(s, first).wait()
            at = lanes_of((PROPS, WINDOW)) + (first - off)
            pick = at == lax.broadcasted_iota(jnp.int32, (PROPS, WINDOW), 0)
            new = dot_tn(fresh_ref[s], jnp.where(pick, 1.0, 0.0).astype(bf16))[0:LINES]
            line = lanes_of((LINES, WINDOW)) + (first - off)
            old = buffer[s].astype(f32)
            buffer[s] = jnp.where((line >= 0) & (line < PROPS), new, old).astype(bf16)
            write(s, first).start()

        return carry

    def end(s, carry):
        _, hit, first = where_is(s)

        @pl.when(hit)
        def _():
            write(s, first).wait()

        return carry

    lax.fori_loop(0, SEQS, begin, 0)
    lax.fori_loop(0, SEQS, change, 0)
    lax.fori_loop(0, SEQS, end, 0)


def place(numbers, cache, fresh, so_far):
    return pl.pallas_call(
        place_kernel,
        out_shape=jax.ShapeDtypeStruct(cache.shape, cache.dtype),
        in_specs=[smem_spec(), any_spec(), vmem_spec(), any_spec()],
        out_specs=any_spec(),
        scratch_shapes=[
            VMEM((SEQS, LINES, WINDOW), bf16),
            pltpu.SemaphoreType.DMA((SEQS,)),
            pltpu.SemaphoreType.DMA((SEQS,)),
        ],
        input_output_aliases={3: 0},
        cost_estimate=cost(1e9, 2e6),
        compiler_params=pltpu.CompilerParams(vmem_limit_bytes=40 << 20),
        name="place",
    )(numbers, cache, fresh, so_far)


def ancestry(parents):
    _, prop_count = parents.shape
    slot_ids = jnp.arange(prop_count, dtype=jnp.int32)
    parent_links = (parents[:, :, None] == slot_ids[None, None, :]).astype(f32)
    identity = jnp.broadcast_to(jnp.eye(prop_count, dtype=f32), parent_links.shape)
    reached = jnp.minimum(identity + parent_links, 1.0)
    for _ in range((prop_count - 1).bit_length()):
        reached = jnp.minimum(
            jnp.einsum("sij,sjk->sik", reached, reached, precision=lax.Precision.HIGHEST), 1.0
        )
    depths = (jnp.sum(reached, axis=-1) - 1.0).astype(jnp.int32)
    return (reached, depths)


def exchange(value, axis):
    return lax.all_to_all(value, axis, 0, 0, tiled=True)


def layer(
    activations,
    latent_cache,
    lengths,
    accepted,
    parents,
    w_query_down,
    w_key_down,
    gain_input,
    gain_query,
    gain_key,
    w_query,
    w_value,
    w_out,
    gain_output,
):
    j = lax.axis_index("kv")
    t = lax.axis_index("tp")
    mine = t[None].astype(jnp.int32)
    cache = jnp.transpose(latent_cache, (0, 2, 1))

    x = pack(jnp.transpose(activations), w_query_down, w_key_down, gain_input.astype(f32)[None])
    x = exchange(x, ALL).reshape(2048, 128)
    y = exchange(down(x), "tp")

    reached, depths = ancestry(parents)
    filled = lengths + accepted
    my_depths = lax.dynamic_slice_in_dim(depths, j, 1, 1)[:, 0]
    half = ROPE_DIM // 2
    frequency = ROPE_BASE ** (-jnp.arange(half, dtype=f32) / half)
    angles = (filled + my_depths).astype(f32)[:, None] * frequency[None, :]
    cosine, sine = jnp.cos(angles), jnp.sin(angles)
    nothing = jnp.zeros((SEQS, 96), f32)
    cosine = jnp.concatenate([cosine, cosine, nothing], axis=1)
    sine = jnp.concatenate([-sine, sine, nothing], axis=1)
    numbers = jnp.concatenate([filled - j * SPAN, t[None]]).astype(jnp.int32)
    group = lax.dynamic_index_in_dim(reached.reshape(3, 8, PROPS, PROPS), t, 1, False)
    anc = jnp.repeat(jnp.pad(group, ((0, 0), (0, 0), (0, 112))), 8, axis=1)

    wq = jnp.transpose(w_query, (1, 2, 0))
    wv = jnp.transpose(w_value, (0, 2, 1))
    z = queries(
        mine,
        y,
        gain_query.astype(f32).reshape(4, 128),
        gain_key.astype(f32).reshape(2, 128),
        cosine,
        sine,
        wq,
    )
    z = exchange(z, ALL)
    sent, fresh = attend(numbers, z, cache, anc, wv)

    updated = None
    for n in range(len(CUTS) - 1):
        updated = copy_cache(cache, updated, CUTS[n], CUTS[n + 1])
    updated = place(numbers, cache, fresh, updated)

    w_here = [w_out]
    for k in range(1, 8):
        w_here.append(lax.ppermute(w_out, "tp", [(n, (n + k) % 8) for n in range(8)]))
    attended = combine(exchange(sent, "kv"))
    mixed, squares = mix(mine, exchange(attended, "kv"), w_here)
    squares = exchange(squares, "kv")
    result = finish(mixed, squares, gain_output.astype(f32)[None])
    result = spread(exchange(result, "tp"))
    return (result, jnp.transpose(updated, (0, 2, 1)))


CUTS = (0, 5, 9, 20, 24)


def solution(mesh):
    return jax.shard_map(
        layer,
        mesh=mesh,
        in_specs=(
            P(None, ALL),
            P(None, "kv", None),
            P(),
            P(),
            P(),
            P(ALL, None),
            P(ALL, None),
            P(ALL),
            P(),
            P(),
            P(None, "tp", None),
            P(),
            P("tp", "kv"),
            P("kv"),
        ),
        out_specs=(P(None, "kv"), P(None, "kv", None)),
        check_vma=False,
    )
```

time: 209 us -> 134 us (0.64)
  matrix products: 59.9 us -> 1.47 us
  Pallas kernels: 0 us -> 40.6 us
  blocking collectives: 38.1 us -> 0 us
  local copies, waits for them, and re-layouts: 27 us -> 4.09 us
  starting transfers between devices: 30.5 us -> 48.7 us
  waiting for transfers between devices: 41 us -> 33.4 us
  other arithmetic: 9.9 us -> 3.17 us
    dot_general x9 -> x0, matrix products: 58.4 us -> none  [the longest x1 25.2 us: local(): jnp.einsum('snj,sja->sna', onehot.astype(jnp.bfloat16), fresh_block, pref...]
    pallas_call x0 -> x13, Pallas kernels: none -> 40.6 us  [the longest x4 22.5 us: copy_cache(): pl.pallas_call(kernel, out_shape=jax.ShapeDtypeStruct(cache.shape, cache....]
    all_to_all x3 -> x0, blocking collectives: 20.4 us -> none  [the longest x2 15.7 us: copy_for_each(): lax.all_to_all(jnp.broadcast_to(value[None], (length, *value.shape)), axi...]
    psum x2 -> x0, blocking collectives: 17.7 us -> none  [one_axis_at_a_time(): return functools.reduce(lax.psum, axes, value)]
    ppermute x0 -> x7, starting transfers between devices: none -> 9.82 us  [layer(): lax.ppermute(w_out, 'tp', [(n, (n + k) % 8) for n in range(8)])]
    all_to_all x5 -> x7, starting transfers between devices: 30.5 us -> 38.9 us  [exchange(): return lax.all_to_all(value, axis, 0, 0, tiled=True)]
    all_to_all x5 -> x7, waiting for transfers between devices: 41 us -> 33.4 us  [exchange(): return lax.all_to_all(value, axis, 0, 0, tiled=True)]
    slice x5 -> x0, local copies, waits for them, and re-layouts: 5.69 us -> none  [the longest x3 5.47 us: together(): outs.append(subtotal[at:at + a.size].reshape(a.shape))]
  transfers between devices with their start and end apart: 5 -> 14, of which waited for: 4 -> 6; matrix products, arithmetic and copies ran while one was open for 12% -> 4% of each run, Pallas kernels for 0% -> 29%
where the time goes in v1:
time: 134 us; the launch traced here: 132 us
  starting transfers between devices  48.7 us (36%)
  Pallas kernels  40.6 us (30%)
  waiting for transfers between devices  33.4 us (25%)
  local copies, waits for them, and re-layouts  4.09 us (3%)
  other arithmetic  3.17 us (2%)
  matrix products  1.47 us (1%)
    all_to_all x7, starting transfers between devices, exchange(): return lax.all_to_all(value, axis, 0, 0, tiled=True)  38.9 us
    all_to_all x7, waiting for transfers between devices, exchange(): return lax.all_to_all(value, axis, 0, 0, tiled=True)  33.4 us
    pallas_call x4, Pallas kernels, copy_cache(): pl.pallas_call(kernel, out_shape=jax.ShapeDtypeStruct(cache.shape, cache....  22.5 us
    ppermute x7, starting transfers between devices, layer(): lax.ppermute(w_out, 'tp', [(n, (n + k) % 8) for n in range(8)])  9.82 us
    pallas_call x1, Pallas kernels, attend(): pl.pallas_call(attend_kernel, out_shape=(jax.ShapeDtypeStruct((16, 32, 12...  8.78 us
    unnamed x15, local copies, waits for them, and re-layouts  3.98 us
  transfers between devices with their start and end apart: 14, of which 6 were waited for; matrix products, arithmetic and copies ran while one was open for 4% of the time, Pallas kernels for 29%

profile of v1, /device:TPU:0, one launch (start us, length us, event | category | flops | bytes accessed | tf_op | source)
XLA Modules:
  0.0 132.4 jit_solution(7049071362475458170)
XLA Ops:
  0.6 3.2 %collective-permute-start.5 = (bf16[128,128]{1,0:T(8,128)(2,1)}, bf16[128,128]{1,0:T(8,128)(2,1)S(1)}, u32[]{:S(2)}, u32[]{:S(2)}) collective-permute-start(bf16[128,128]{1,0:T(8,128)(2,1)} %refs_0_.1), channel_id=1, source_target_pairs={{0,6},{1,7},{2,0},{3,1},{4,2},{5,3},{6,4},{7,5},{8,14},{9,15},{10,... | collective-permute-start | bytes 98312 | tf_op jit(solution)/shard_map/ppermute | solution.py:643
  3.8 2.7 %collective-permute-start.3 = (bf16[128,128]{1,0:T(8,128)(2,1)}, bf16[128,128]{1,0:T(8,128)(2,1)S(1)}, u32[]{:S(2)}, u32[]{:S(2)}) collective-permute-start(bf16[128,128]{1,0:T(8,128)(2,1)} %refs_0_.1), channel_id=1, source_target_pairs={{0,4},{1,5},{2,6},{3,7},{4,0},{5,1},{6,2},{7,3},{8,12},{9,13},{10,... | collective-permute-start | bytes 98312 | tf_op jit(solution)/shard_map/ppermute | solution.py:643
  6.5 1.0 collective-permute-start.1
  8.2 0.7 copy-done.3
  10.3 1.1 shard_map.149
  11.4 10.4 %all-to-all-start = ((bf16[128,16,128]{2,1,0:T(8,128)(2,1)}), bf16[128,16,128]{2,1,0:T(8,128)(2,1)S(1)}, u32[]{:S(2)}, u32[]{:S(2)}) async-start(bf16[128,16,128]{2,1,0:T(8,128)(2,1)} %shard_map.149), calls=%async_computation | async-start | bytes 1048576 | tf_op jit(solution)/shard_map/all_to_all | solution.py:580
  22.5 0.8 copy.22
  26.0 9.3 %all-to-all-done = bf16[128,16,128]{2,1,0:T(8,128)(2,1)S(1)} async-done(((bf16[128,16,128]{2,1,0:T(8,128)(2,1)}), bf16[128,16,128]{2,1,0:T(8,128)(2,1)S(1)}, u32[]{:S(2)}, u32[]{:S(2)}) %all-to-all-start) | async-done | bytes 524320 | tf_op jit(solution)/shard_map/all_to_all | solution.py:580
  35.3 1.4 %shard_map.150 = f32[8,24,128]{2,1,0:T(8,128)} custom-call(bf16[2048,128]{1,0:T(8,128)(2,1)S(1)} %bitcast.30), custom_call_target="tpu_custom_call" | custom-call | flops 67108864 | bytes 524288 | tf_op jit(solution)/shard_map/pallas_call | solution.py:126
  36.6 3.4 %all-to-all-start.1 = ((f32[8,24,128]{2,1,0:T(8,128)}), f32[8,24,128]{2,1,0:T(8,128)S(1)}, u32[]{:S(2)}, u32[]{:S(2)}) async-start(f32[8,24,128]{2,1,0:T(8,128)} %shard_map.150), calls=%async_computation.1 | async-start | bytes 196608 | tf_op jit(solution)/shard_map/all_to_all | solution.py:580
  40.7 5.1 %all-to-all-done.1.y_ref = f32[8,24,128]{2,1,0:T(8,128)S(1)} async-done(((f32[8,24,128]{2,1,0:T(8,128)}), f32[8,24,128]{2,1,0:T(8,128)S(1)}, u32[]{:S(2)}, u32[]{:S(2)}) %all-to-all-start.1) | async-done | bytes 98336 | tf_op jit(solution)/shard_map/all_to_all | solution.py:580
  45.7 1.1 copy-done
  46.8 1.5 %queries.1 = bf16[128,24,128]{2,1,0:T(8,128)(2,1)} custom-call(s32[1]{0:T(128)} %bitcast.t_ref, f32[8,24,128]{2,1,0:T(8,128)S(1)} %all-to-all-done.1.y_ref, f32[4,128]{1,0:T(4,128)S(1)} %bitcast_convert_fusion.gq_ref, f32[2,128]{1,0:T(2,128)S(1)} %bitcast_convert_fusion.2.gk_ref, f32[24,128]{1,0:T(8,128)S(1)} %get-tuple-element.16.cos_ref, ...), custom_call_target="tpu_custom_call" | custom-call | flops 14155776 | bytes 786432 | tf_op jit(solution)/shard_map/queries/pallas_call | solution.py:204
  48.3 4.8 %all-to-all-start.2 = ((bf16[128,24,128]{2,1,0:T(8,128)(2,1)}), bf16[128,24,128]{2,1,0:T(8,128)(2,1)S(1)}, u32[]{:S(2)}, u32[]{:S(2)}) async-start(bf16[128,24,128]{2,1,0:T(8,128)(2,1)} %queries.1), calls=%async_computation.2 | async-start | bytes 1572864 | tf_op jit(solution)/shard_map/all_to_all | solution.py:580
  53.2 5.2 %copy_cache.4.refs_1_ = bf16[24,288,2048]{2,1,0:T(8,128)(2,1)} custom-call(bf16[24,288,2048]{2,1,0:T(8,128)(2,1)} %bitcast.34), custom_call_target="tpu_custom_call" | custom-call | flops 4499999744 | bytes 11796480 | tf_op jit(solution)/shard_map/copy_cache/pallas_call | solution.py:470
  58.4 3.9 %copy_cache.5.refs_1_ = bf16[24,288,2048]{2,1,0:T(8,128)(2,1)} custom-call(bf16[24,288,2048]{2,1,0:T(8,128)(2,1)} %bitcast.35, bf16[24,288,2048]{2,1,0:T(8,128)(2,1)} %copy_cache.4.refs_1_), custom_call_target="tpu_custom_call", output_to_operand_aliasing={{}: (1, {})} | custom-call | flops 3600000000 | bytes 9437184 | tf_op jit(solution)/shard_map/copy_cache/pallas_call | solution.py:470
  62.3 6.9 %all-to-all-done.2.z_ref = bf16[128,24,128]{2,1,0:T(8,128)(2,1)S(1)} async-done(((bf16[128,24,128]{2,1,0:T(8,128)(2,1)}), bf16[128,24,128]{2,1,0:T(8,128)(2,1)S(1)}, u32[]{:S(2)}, u32[]{:S(2)}) %all-to-all-start.2) | async-done | bytes 786464 | tf_op jit(solution)/shard_map/all_to_all | solution.py:580
  69.2 8.8 %attend.1 = (bf16[16,32,128]{2,1,0:T(8,128)(2,1)}, bf16[24,16,384]{2,1,0:T(8,128)(2,1)S(1)}) custom-call(s32[25]{0:T(128)S(1)} %pad_add_fusion.n_ref, bf16[128,24,128]{2,1,0:T(8,128)(2,1)S(1)} %all-to-all-done.2.z_ref, bf16[24,288,2048]{2,1,0:T(8,128)(2,1)} %bitcast.36, f32[3,128,128]{2,1,0:T(8,128)S(1)} %broadcast_bitcast_fusion.anc_ref, ...), custom_call_target="tpu_custom_call" | custom-call | flops 1711276032 | bytes 3538944 | tf_op jit(solution)/shard_map/attend/pallas_call | solution.py:319
  78.0 3.5 %all-to-all-start.3 = ((bf16[16,32,128]{2,1,0:T(8,128)(2,1)}), bf16[16,32,128]{2,1,0:T(8,128)(2,1)S(1)}, u32[]{:S(2)}, u32[]{:S(2)}) async-start(bf16[16,32,128]{2,1,0:T(8,128)(2,1)} %get-tuple-element.6), calls=%async_computation.3 | async-start | bytes 262144 | tf_op jit(solution)/shard_map/all_to_all | solution.py:580
  81.5 9.5 %copy_cache.6.refs_1_ = bf16[24,288,2048]{2,1,0:T(8,128)(2,1)} custom-call(bf16[24,288,2048]{2,1,0:T(8,128)(2,1)} %bitcast.37, bf16[24,288,2048]{2,1,0:T(8,128)(2,1)} %copy_cache.5.refs_1_), custom_call_target="tpu_custom_call", output_to_operand_aliasing={{}: (1, {})} | custom-call | flops 9900000256 | bytes 25952256 | tf_op jit(solution)/shard_map/copy_cache/pallas_call | solution.py:470
  91.1 0.9 shard_map.151
  92.0 7.2 %all-to-all-start.4 = ((bf16[16,24,128]{2,1,0:T(8,128)(2,1)}), bf16[16,24,128]{2,1,0:T(8,128)(2,1)S(1)}, u32[]{:S(2)}, u32[]{:S(2)}) async-start(bf16[16,24,128]{2,1,0:T(8,128)(2,1)} %shard_map.151), calls=%async_computation.4 | async-start | bytes 196608 | tf_op jit(solution)/shard_map/all_to_all | solution.py:580
  99.3 2.9 %collective-permute-start.6 = (bf16[128,128]{1,0:T(8,128)(2,1)S(1)}, bf16[128,128]{1,0:T(8,128)(2,1)S(1)}, u32[]{:S(2)}, u32[]{:S(2)}) collective-permute-start(bf16[128,128]{1,0:T(8,128)(2,1)S(1)} %copy-done.2), channel_id=1, source_target_pairs={{0,7},{1,0},{2,1},{3,2},{4,3},{5,4},{6,5},{7,6},{8,15},{9,8},{10,9... | collective-permute-start | bytes 98312 | tf_op jit(solution)/shard_map/ppermute | solution.py:643
  102.2 3.8 %copy_cache.7.old_ref = bf16[24,288,2048]{2,1,0:T(8,128)(2,1)} custom-call(bf16[24,288,2048]{2,1,0:T(8,128)(2,1)} %bitcast.38, bf16[24,288,2048]{2,1,0:T(8,128)(2,1)} %copy_cache.6.refs_1_), custom_call_target="tpu_custom_call", output_to_operand_aliasing={{}: (1, {})} | custom-call | flops 3600000000 | bytes 9437184 | tf_op jit(solution)/shard_map/copy_cache/pallas_call | solution.py:470
  106.1 0.9 all-to-all-done.4.u_ref
  107.0 1.0 mix.1
  108.0 6.3 %all-to-all-start.5 = ((f32[16,8,128]{2,1,0:T(8,128)}), f32[16,8,128]{2,1,0:T(8,128)S(1)}, u32[]{:S(2)}, u32[]{:S(2)}) async-start(f32[16,8,128]{2,1,0:T(8,128)} %get-tuple-element.8), calls=%async_computation.5 | async-start | bytes 131072 | tf_op jit(solution)/shard_map/all_to_all | solution.py:580
  114.3 7.6 %all-to-all-done.5.s_ref = f32[16,8,128]{2,1,0:T(8,128)S(1)} async-done(((f32[16,8,128]{2,1,0:T(8,128)}), f32[16,8,128]{2,1,0:T(8,128)S(1)}, u32[]{:S(2)}, u32[]{:S(2)}) %all-to-all-start.5) | async-done | bytes 65568 | tf_op jit(solution)/shard_map/all_to_all | solution.py:580
  122.0 0.8 shard_map.152
  122.7 3.4 %all-to-all-start.6 = ((bf16[8,48,128]{2,1,0:T(8,128)(2,1)}), bf16[8,48,128]{2,1,0:T(8,128)(2,1)S(1)}, u32[]{:S(2)}, u32[]{:S(2)}) async-start(bf16[8,48,128]{2,1,0:T(8,128)(2,1)} %shard_map.152), calls=%async_computation.6 | async-start | bytes 196608 | tf_op jit(solution)/shard_map/all_to_all | solution.py:580
  126.1 2.1 %place.1 = bf16[24,288,2048]{2,1,0:T(8,128)(2,1)} custom-call(s32[25]{0:T(128)S(1)} %pad_add_fusion.n_ref, bf16[24,288,2048]{2,1,0:T(8,128)(2,1)} %bitcast.39, bf16[24,16,384]{2,1,0:T(8,128)(2,1)S(1)} %get-tuple-element.9.fresh_ref, bf16[24,288,2048]{2,1,0:T(8,128)(2,1)} %copy_cache.7.old_ref), custom_call_target="tpu_custom_call", output_to_operand_aliasing={{}: (3, {})} | custom-call | flops 1000000000 | bytes 2000000 | tf_op jit(solution)/shard_map/place/pallas_call | solution.py:548
  128.2 3.6 %all-to-all-done.6.m_ref = bf16[8,48,128]{2,1,0:T(8,128)(2,1)S(1)} async-done(((bf16[8,48,128]{2,1,0:T(8,128)(2,1)}), bf16[8,48,128]{2,1,0:T(8,128)(2,1)S(1)}, u32[]{:S(2)}, u32[]{:S(2)}) %all-to-all-start.6) | async-done | bytes 98336 | tf_op jit(solution)/shard_map/all_to_all | solution.py:580
  (44 shorter events, 6.9 us)
Async XLA Ops:
  0.6 98.6 %collective-permute-start.5 = (bf16[128,128]{1,0:T(8,128)(2,1)}, bf16[128,128]{1,0:T(8,128)(2,1)S(1)}, u32[]{:S(2)}, u32[]{:S(2)}) collective-permute-start(bf16[128,128]{1,0:T(8,128)(2,1)} %refs_0_.1), channel_id=1, source_target_pairs={{0,6},{1,7},{2,0},{3,1},{4,2},{5,3},{6,4},{7,5},{8,14},{9,15},{10,... | collective-permute-start | bytes 98312 | tf_op jit(solution)/shard_map/ppermute | solution.py:643
  3.8 95.4 %collective-permute-start.4 = (bf16[128,128]{1,0:T(8,128)(2,1)}, bf16[128,128]{1,0:T(8,128)(2,1)S(1)}, u32[]{:S(2)}, u32[]{:S(2)}) collective-permute-start(bf16[128,128]{1,0:T(8,128)(2,1)} %refs_0_.1), channel_id=1, source_target_pairs={{0,5},{1,6},{2,7},{3,0},{4,1},{5,2},{6,3},{7,4},{8,13},{9,14},{10,... | collective-permute-start | bytes 98312 | tf_op jit(solution)/shard_map/ppermute | solution.py:643
  3.8 102.2 %collective-permute-start.3 = (bf16[128,128]{1,0:T(8,128)(2,1)}, bf16[128,128]{1,0:T(8,128)(2,1)S(1)}, u32[]{:S(2)}, u32[]{:S(2)}) collective-permute-start(bf16[128,128]{1,0:T(8,128)(2,1)} %refs_0_.1), channel_id=1, source_target_pairs={{0,4},{1,5},{2,6},{3,7},{4,0},{5,1},{6,2},{7,3},{8,12},{9,13},{10,... | collective-permute-start | bytes 98312 | tf_op jit(solution)/shard_map/ppermute | solution.py:643
  6.5 99.5 %collective-permute-start.2 = (bf16[128,128]{1,0:T(8,128)(2,1)}, bf16[128,128]{1,0:T(8,128)(2,1)S(1)}, u32[]{:S(2)}, u32[]{:S(2)}) collective-permute-start(bf16[128,128]{1,0:T(8,128)(2,1)} %refs_0_.1), channel_id=1, source_target_pairs={{0,3},{1,4},{2,5},{3,6},{4,7},{5,0},{6,1},{7,2},{8,11},{9,12},{10,... | collective-permute-start | bytes 98312 | tf_op jit(solution)/shard_map/ppermute | solution.py:643
  6.5 99.5 %collective-permute-start.1 = (bf16[128,128]{1,0:T(8,128)(2,1)}, bf16[128,128]{1,0:T(8,128)(2,1)S(1)}, u32[]{:S(2)}, u32[]{:S(2)}) collective-permute-start(bf16[128,128]{1,0:T(8,128)(2,1)} %refs_0_.1), channel_id=1, source_target_pairs={{0,2},{1,3},{2,4},{3,5},{4,6},{5,7},{6,0},{7,1},{8,10},{9,11},{10,... | collective-permute-start | bytes 98312 | tf_op jit(solution)/shard_map/ppermute | solution.py:643
  8.2 0.7 copy-start.3
  8.9 0.7 copy-start.4
  9.6 0.7 copy-start.5
  11.4 23.9 %all-to-all-start = ((bf16[128,16,128]{2,1,0:T(8,128)(2,1)}), bf16[128,16,128]{2,1,0:T(8,128)(2,1)S(1)}, u32[]{:S(2)}, u32[]{:S(2)}) async-start(bf16[128,16,128]{2,1,0:T(8,128)(2,1)} %shard_map.149), calls=%async_computation | async-start | bytes 1048576 | tf_op jit(solution)/shard_map/all_to_all | solution.py:580
  36.6 9.1 %all-to-all-start.1 = ((f32[8,24,128]{2,1,0:T(8,128)}), f32[8,24,128]{2,1,0:T(8,128)S(1)}, u32[]{:S(2)}, u32[]{:S(2)}) async-start(f32[8,24,128]{2,1,0:T(8,128)} %shard_map.150), calls=%async_computation.1 | async-start | bytes 196608 | tf_op jit(solution)/shard_map/all_to_all | solution.py:580
  45.7 1.1 copy-start
  48.3 20.9 %all-to-all-start.2 = ((bf16[128,24,128]{2,1,0:T(8,128)(2,1)}), bf16[128,24,128]{2,1,0:T(8,128)(2,1)S(1)}, u32[]{:S(2)}, u32[]{:S(2)}) async-start(bf16[128,24,128]{2,1,0:T(8,128)(2,1)} %queries.1), calls=%async_computation.2 | async-start | bytes 1572864 | tf_op jit(solution)/shard_map/all_to_all | solution.py:580
  58.4 10.8 %copy-start.1 = (bf16[16,256,64]{1,2,0:T(8,128)(2,1)S(1)}, bf16[16,256,64]{1,2,0:T(8,128)(2,1)}, u32[]{:S(2)}) copy-start(bf16[16,256,64]{1,2,0:T(8,128)(2,1)} %param.25) | copy-start | bytes 1572868
  78.0 13.1 %all-to-all-start.3 = ((bf16[16,32,128]{2,1,0:T(8,128)(2,1)}), bf16[16,32,128]{2,1,0:T(8,128)(2,1)S(1)}, u32[]{:S(2)}, u32[]{:S(2)}) async-start(bf16[16,32,128]{2,1,0:T(8,128)(2,1)} %get-tuple-element.6), calls=%async_computation.3 | async-start | bytes 262144 | tf_op jit(solution)/shard_map/all_to_all | solution.py:580
  81.5 17.7 %copy-start.2 = (bf16[128,128]{1,0:T(8,128)(2,1)S(1)}, bf16[128,128]{1,0:T(8,128)(2,1)}, u32[]{:S(2)}) copy-start(bf16[128,128]{1,0:T(8,128)(2,1)} %refs_0_.1) | copy-start | bytes 98308
  92.0 15.0 %all-to-all-start.4 = ((bf16[16,24,128]{2,1,0:T(8,128)(2,1)}), bf16[16,24,128]{2,1,0:T(8,128)(2,1)S(1)}, u32[]{:S(2)}, u32[]{:S(2)}) async-start(bf16[16,24,128]{2,1,0:T(8,128)(2,1)} %shard_map.151), calls=%async_computation.4 | async-start | bytes 196608 | tf_op jit(solution)/shard_map/all_to_all | solution.py:580
  99.2 15.1 %copy-start.6 = (bf16[128]{0:T(256)(128)(2,1)S(1)}, bf16[128]{0:T(256)(128)(2,1)}, u32[]{:S(2)}) copy-start(bf16[128]{0:T(256)(128)(2,1)} %param.27) | copy-start | bytes 772
  99.2 6.8 %collective-permute-start = (bf16[128,128]{1,0:T(8,128)(2,1)S(1)}, bf16[128,128]{1,0:T(8,128)(2,1)S(1)}, u32[]{:S(2)}, u32[]{:S(2)}) collective-permute-start(bf16[128,128]{1,0:T(8,128)(2,1)S(1)} %copy-done.2), channel_id=1, source_target_pairs={{0,1},{1,2},{2,3},{3,4},{4,5},{5,6},{6,7},{7,0},{8,9},{9,10},{10,1... | collective-permute-start | bytes 98312 | tf_op jit(solution)/shard_map/ppermute | solution.py:643
  99.3 6.8 %collective-permute-start.6 = (bf16[128,128]{1,0:T(8,128)(2,1)S(1)}, bf16[128,128]{1,0:T(8,128)(2,1)S(1)}, u32[]{:S(2)}, u32[]{:S(2)}) collective-permute-start(bf16[128,128]{1,0:T(8,128)(2,1)S(1)} %copy-done.2), channel_id=1, source_target_pairs={{0,7},{1,0},{2,1},{3,2},{4,3},{5,4},{6,5},{7,6},{8,15},{9,8},{10,9... | collective-permute-start | bytes 98312 | tf_op jit(solution)/shard_map/ppermute | solution.py:643
  108.0 14.0 %all-to-all-start.5 = ((f32[16,8,128]{2,1,0:T(8,128)}), f32[16,8,128]{2,1,0:T(8,128)S(1)}, u32[]{:S(2)}, u32[]{:S(2)}) async-start(f32[16,8,128]{2,1,0:T(8,128)} %get-tuple-element.8), calls=%async_computation.5 | async-start | bytes 131072 | tf_op jit(solution)/shard_map/all_to_all | solution.py:580
  122.7 9.1 %all-to-all-start.6 = ((bf16[8,48,128]{2,1,0:T(8,128)(2,1)}), bf16[8,48,128]{2,1,0:T(8,128)(2,1)S(1)}, u32[]{:S(2)}, u32[]{:S(2)}) async-start(bf16[8,48,128]{2,1,0:T(8,128)(2,1)} %shard_map.152), calls=%async_computation.6 | async-start | bytes 196608 | tf_op jit(solution)/shard_map/all_to_all | solution.py:580

commit v2 on v1

--- a/solution.py
+++ b/solution.py
@@ -13,6 +13,7 @@
 SEQS = 24
 PROPS = 16
 SPAN = 2048
+KV_RANK = 256
 ROPE_DIM = 32
 LINES = 288
 SCALE = 96.0 ** (-0.5)
@@ -82,7 +83,7 @@
     pick = jnp.where(lanes_of((384, 512)) == place, 1.0, 0.0).astype(bf16)
     lines = dot_nn(a_ref[...], pick)
     lane = lanes_of((16, 128))
-    gain = jnp.broadcast_to(g_ref[...], (16, 16))
+    gain = jnp.broadcast_to(g_ref[...].astype(f32), (16, 16))
     diagonal = lax.broadcasted_iota(jnp.int32, (16, 16), 0) == lanes_of((16, 16))
     gain = jnp.sum(jnp.where(diagonal, gain, 0.0), axis=1, keepdims=True)
     query = q_ref[...].astype(f32)
@@ -105,7 +106,7 @@
 
 def pack(a, q, k, g):
     return call(
-        pack_kernel, jax.ShapeDtypeStruct((128, 16, 128), bf16), 4, cost(1e8, 1e6)
+        pack_kernel, jax.ShapeDtypeStruct((128, 16, 128), bf16), 4, cost(1e8, 1e6), limit=60
     )(a, q, k, g)
 
 
@@ -214,10 +215,25 @@
 
 
 CHUNK = 512
+LOG2E = 1.4426950408889634
 
 
 def attend_kernel(
-    n_ref, z_ref, cache_ref, anc_ref, wv_ref, o_ref, fresh_ref, keys, wide, lines, part, lam, score, sems
+    n_ref,
+    z_ref,
+    cache_ref,
+    anc_ref,
+    wv_ref,
+    o_ref,
+    fresh_ref,
+    keys,
+    wide,
+    lines,
+    part,
+    lam,
+    score,
+    prob,
+    sems,
 ):
     mine = n_ref[24]
 
@@ -249,53 +265,78 @@
         for t in range(8):
             fresh_ref[s * 8 + t] = fresh_of(s, t)
     slot = lanes_of((256, 16))
-    for s in range(3):
+
+    def tiles(v, join):
+        out = v[:, 0:128]
+        for n in range(1, v.shape[1] // 128):
+            out = join(out, v[:, n * 128 : n * 128 + 128])
+        return out
+
+    def scores(s):
         off = n_ref[s * 8 + mine]
-        fresh = fresh_of(s, mine)
-        lat = jnp.concatenate(
+        fresh = fresh_of(s, mine)[:, 0:LINES]
+        query = jnp.concatenate(
             [
                 jnp.concatenate(
-                    [wide[:, (s * 2 + hh) * 2, :], wide[:, (s * 2 + hh) * 2 + 1, :]], axis=1
+                    [
+                        wide[:, (s * 2 + hh) * 2, :],
+                        wide[:, (s * 2 + hh) * 2 + 1, :],
+                        rope_of(s * 2 + hh)[:, 0:ROPE_DIM],
+                    ],
+                    axis=1,
                 )
                 for hh in range(2)
             ],
             axis=0,
         ).astype(bf16)
-        rope = jnp.concatenate([rope_of(s * 2 + hh)[:, 0:32] for hh in range(2)], axis=0).astype(
-            bf16
-        )
-        near = (dot_nt(lat, fresh[:, 0:256]) + dot_nt(rope, fresh[:, 256:288])) * SCALE
+        near = dot_nt(query, fresh) * (SCALE * LOG2E)
         anc = anc_ref[s][:, 0:16]
         seen = (
             (jnp.concatenate([anc, anc], axis=0) > 0.5) & (slot + off >= 0) & (slot + off < SPAN)
         )
         near = jnp.where(seen, near, MASKED)
-        top = jnp.max(near, axis=1, keepdims=True)
-        fetch(s).wait()
+        most = None
         for c in range(SPAN // CHUNK):
             cols = slice(c * CHUNK, (c + 1) * CHUNK)
-            got = (
-                dot_nn(lat, keys[s, 0:256, cols]) + dot_nn(rope, keys[s, 256:288, cols])
-            ) * SCALE
-            got = jnp.where(lanes_of(got.shape) + c * CHUNK < off, got, MASKED)
-            score[:, cols] = got
-            top = jnp.maximum(top, jnp.max(got, axis=1, keepdims=True))
-        weight = jnp.where(seen, jnp.exp(near - top), 0.0)
+            bias = jnp.where(lanes_of((1, CHUNK)) + c * CHUNK < off, 0.0, MASKED)
+            got = dot_nn(query, keys[s, :, cols]) * (SCALE * LOG2E) + bias
+            score[s, :, cols] = got
+            got = tiles(got, jnp.maximum)
+            most = got if most is None else jnp.maximum(most, got)
+        top = jnp.maximum(
+            jnp.max(most, axis=1, keepdims=True), jnp.max(near, axis=1, keepdims=True)
+        )
+        return fresh, near, top
+
+    def values(s, fresh, near, top):
+        base = jnp.where(top < 0.1 * MASKED, 0.0, top)
+        weight = jnp.exp2(near - base)
         total = jnp.sum(weight, axis=1, keepdims=True)
-        acc = dot_nn(weight.astype(bf16), fresh[:, 0:256])
+        acc = dot_nn(weight.astype(bf16), fresh[:, 0:KV_RANK])
+        count = None
         for c in range(SPAN // CHUNK):
             cols = slice(c * CHUNK, (c + 1) * CHUNK)
-            got = score[:, cols]
-            weight = jnp.where(
-                lanes_of(got.shape) + c * CHUNK < off, jnp.exp(got - top), 0.0
-            )
-            total = total + jnp.sum(weight, axis=1, keepdims=True)
-            acc = acc + dot_nt(weight.astype(bf16), keys[s, 0:256, cols])
+            weight = jnp.exp2(score[s, :, cols] - base)
+            prob[s, :, cols] = weight.astype(bf16)
+            weight = tiles(weight, jnp.add)
+            count = weight if count is None else count + weight
+        total = total + jnp.sum(count, axis=1, keepdims=True)
+        acc = acc + dot_nt(prob[s], keys[s, 0:KV_RANK, :])
         acc = rounded(acc / jnp.maximum(total, 1.0))
         for half in range(2):
             part[s, half] = acc[:, half * 128 : half * 128 + 128]
-        level = jnp.where(total > 0.0, top + jnp.log(jnp.maximum(total, 1.0)), MASKED)
+        level = jnp.where(total > 0.0, top + jnp.log2(jnp.maximum(total, 1.0)), MASKED)
         lam[s] = jnp.broadcast_to(level, (256, 128))
+
+    fetch(0).wait()
+    first = scores(0)
+    fetch(1).wait()
+    fetch(2).wait()
+    second = scores(1)
+    values(0, *first)
+    third = scores(2)
+    values(1, *second)
+    values(2, *third)
     small = lanes_of((8, 128))
     for h in range(16):
         pieces = []
@@ -330,11 +371,12 @@
             VMEM((3, 3, 128, 128), f32),
             VMEM((3, 2, 256, 128), f32),
             VMEM((3, 256, 128), f32),
-            VMEM((256, SPAN), f32),
+            VMEM((3, 256, SPAN), f32),
+            VMEM((3, 256, SPAN), bf16),
             pltpu.SemaphoreType.DMA((3,)),
         ],
         cost_estimate=cost(3 * 2 * 256 * 2048 * 544, 3 * LINES * SPAN * 2),
-        compiler_params=pltpu.CompilerParams(vmem_limit_bytes=40 << 20),
+        compiler_params=pltpu.CompilerParams(vmem_limit_bytes=52 << 20),
         name="attend",
     )(numbers, z, cache, anc, wv)
 
@@ -348,7 +390,7 @@
     for s in range(3):
         low, high = (level[:, :, 4 * (h * 3 + s) : 4 * (h * 3 + s) + 1] for h in range(2))
         both = jnp.where(lane < 64, low, high)
-        share = jnp.exp(both - jnp.max(both, axis=0, keepdims=True))
+        share = jnp.exp2(both - jnp.max(both, axis=0, keepdims=True))
         summed = jnp.sum(share * v[:, s * 8 : s * 8 + 8, :], axis=0)
         outs.append(summed / jnp.sum(share, axis=0))
     o_ref[...] = jnp.broadcast_to(jnp.concatenate(outs, axis=0).astype(bf16), o_ref.shape)
@@ -359,16 +401,17 @@
 
 
 def mix_kernel(t_ref, u_ref, *refs):
-    w_refs, (o_ref, s_ref) = refs[:8], refs[8:]
+    w_refs, (o_ref, s_ref) = refs[:4], refs[4:]
     lane = lanes_of((24, 128))
     mixed = jnp.zeros((48, 128), f32)
-    for k in range(8):
-        p = (t_ref[0] - k) & 7
-        a, b = u_ref[2 * p].astype(f32), u_ref[2 * p + 1].astype(f32)
-        left = jnp.where(lane < 64, a, turn(b, 64))
-        right = jnp.where(lane < 64, turn(a, 64), b)
-        lhs = jnp.concatenate([left, right], axis=0).astype(bf16)
-        mixed = mixed + dot_nn(lhs, w_refs[k][...])
+    for k in range(4):
+        for b in range(2):
+            p = ((t_ref[0] - 2 * k) & 7) ^ b
+            first, second = u_ref[2 * p].astype(f32), u_ref[2 * p + 1].astype(f32)
+            left = jnp.where(lane < 64, first, turn(second, 64))
+            right = jnp.where(lane < 64, turn(first, 64), second)
+            lhs = jnp.concatenate([left, right], axis=0).astype(bf16)
+            mixed = mixed + dot_nn(lhs, w_refs[k][b])
     o_ref[...] = mixed
     squares = jnp.broadcast_to(jnp.sum(mixed * mixed, axis=1, keepdims=True), mixed.shape)
     row = lax.broadcasted_iota(jnp.int32, (48, 128), 0)
@@ -381,9 +424,9 @@
         mix_kernel,
         out_shape=(
             jax.ShapeDtypeStruct((48, 128), f32),
-            jax.ShapeDtypeStruct((16, 8, 128), f32),
+            jax.ShapeDtypeStruct((128, 1, 128), f32),
         ),
-        in_specs=[smem_spec()] + [vmem_spec()] * 9,
+        in_specs=[smem_spec()] + [vmem_spec()] * 5,
         out_specs=(vmem_spec(),) * 2,
         cost_estimate=cost(2 * 48 * 1024 * 128, 4e5),
         compiler_params=pltpu.CompilerParams(vmem_limit_bytes=16 << 20),
@@ -391,32 +434,34 @@
     )(t, u, *w)
 
 
-def finish_kernel(m_ref, s_ref, g_ref, o_ref):
-    total = jnp.sum(s_ref[...], axis=0)[0:1]
-    inverse = lax.rsqrt(total / D + EPS)
+def finish_kernel(t_ref, s_ref, g_ref, *refs):
+    m_refs, (o_ref, scale) = refs[:8], refs[8:]
+    scale[...] = lax.rsqrt(jnp.sum(s_ref[...], axis=0) / D + EPS)
     row = lax.broadcasted_iota(jnp.int32, (48, 128), 0)
     same = row == lanes_of((48, 128))
-    column = jnp.sum(jnp.where(same, inverse, 0.0), axis=1, keepdims=True)
-    out = m_ref[...] * column * g_ref[...]
-    rows = []
-    for s in range(3):
-        rows += [out[s * 8 : s * 8 + 8], out[24 + s * 8 : 32 + s * 8]]
-    rows = jnp.concatenate(rows, axis=0).astype(bf16)
-    o_ref[...] = jnp.broadcast_to(rows, o_ref.shape)
-
-
-def finish(m, s, g):
-    return call(finish_kernel, jax.ShapeDtypeStruct((8, 48, 128), bf16), 3, cost(1e6, 4e5))(m, s, g)
-
-
-def spread_kernel(m_ref, o_ref):
-    for t in range(8):
+    gain = g_ref[...]
+    for k in range(8):
+        p = (t_ref[0] - k) & 7
+        inverse = scale[pl.ds(p, 1), :]
+        column = jnp.sum(jnp.where(same, inverse, 0.0), axis=1, keepdims=True)
+        out = m_refs[k][...] * column * gain
         for s in range(3):
-            o_ref[(s * 8 + t) * 16 : (s * 8 + t) * 16 + 16, :] = m_ref[t, s * 16 : s * 16 + 16]
-
-
-def spread(m):
-    return call(spread_kernel, jax.ShapeDtypeStruct((384, 128), bf16), 1, cost(1e6, 4e5))(m)
+            rows = jnp.concatenate([out[s * 8 : s * 8 + 8], out[24 + s * 8 : 32 + s * 8]], axis=0)
+            at = pl.multiple_of((s * 8 + p) * 16, 16)
+            o_ref[pl.ds(at, 16), :] = rows.astype(bf16)
+
+
+def finish(t, s, g, m):
+    return pl.pallas_call(
+        finish_kernel,
+        out_shape=jax.ShapeDtypeStruct((384, 128), bf16),
+        in_specs=[smem_spec()] + [vmem_spec()] * 10,
+        out_specs=vmem_spec(),
+        scratch_shapes=[VMEM((8, 128), f32)],
+        cost_estimate=cost(1e6, 4e5),
+        compiler_params=pltpu.CompilerParams(vmem_limit_bytes=16 << 20),
+        name="finish",
+    )(t, s, g, *m)
 
 
 DEPTH = 4
@@ -601,7 +646,7 @@
     mine = t[None].astype(jnp.int32)
     cache = jnp.transpose(latent_cache, (0, 2, 1))
 
-    x = pack(jnp.transpose(activations), w_query_down, w_key_down, gain_input.astype(f32)[None])
+    x = pack(jnp.transpose(activations), w_query_down, w_key_down, gain_input[None])
     x = exchange(x, ALL).reshape(2048, 128)
     y = exchange(down(x), "tp")
 
@@ -638,18 +683,21 @@
         updated = copy_cache(cache, updated, CUTS[n], CUTS[n + 1])
     updated = place(numbers, cache, fresh, updated)
 
-    w_here = [w_out]
-    for k in range(1, 8):
-        w_here.append(lax.ppermute(w_out, "tp", [(n, (n + k) % 8) for n in range(8)]))
+    def shift(value, distance):
+        return lax.ppermute(value, "tp", [(n, (n + distance) % 8) for n in range(8)])
+
+    other = lax.ppermute(w_out, "tp", [(n, n ^ 1) for n in range(8)])
+    w_here = [jnp.stack([w_out, other])]
+    w_here += [shift(w_here[0], 2 * k) for k in range(1, 4)]
     attended = combine(exchange(sent, "kv"))
     mixed, squares = mix(mine, exchange(attended, "kv"), w_here)
-    squares = exchange(squares, "kv")
-    result = finish(mixed, squares, gain_output.astype(f32)[None])
-    result = spread(exchange(result, "tp"))
+    squares = exchange(squares, ALL).reshape(16, 8, 128)
+    mixed = [mixed] + [shift(mixed, k) for k in range(1, 8)]
+    result = finish(mine, squares, gain_output.astype(f32)[None], mixed)
     return (result, jnp.transpose(updated, (0, 2, 1)))
 
 
-CUTS = (0, 5, 9, 20, 24)
+CUTS = (0, 5, 9, 24)
 
 
 def solution(mesh):

time: 134 us -> 129 us (0.963)
  Pallas kernels: 40.6 us -> 38.3 us
  local copies, waits for them, and re-layouts: 4.09 us -> 1.96 us
    all_to_all x7 -> x6, waiting for transfers between devices: 33.4 us -> 30.4 us  [exchange(): return lax.all_to_all(value, axis, 0, 0, tiled=True)]
    ppermute x7 -> x11, waiting for transfers between devices: 0.02 us -> 2.46 us  [the longest x10 2.46 us: shift(): lax.ppermute(value, 'tp', [(n, (n + distance) % 8) for n in range(8)])]
    unnamed x15 -> x9, local copies, waits for them, and re-layouts: 3.98 us -> 1.85 us
    pallas_call x1, Pallas kernels: 8.78 us -> 7.07 us  [attend(): pl.pallas_call(attend_kernel, out_shape=(jax.ShapeDtypeStruct((16, 32, 12...]
    pallas_call x4 -> x3, Pallas kernels: 22.5 us -> 21.7 us  [copy_cache(): pl.pallas_call(kernel, out_shape=jax.ShapeDtypeStruct(cache.shape, cache....]
    ppermute x7 -> x11, starting transfers between devices: 9.82 us -> 10.3 us  [the longest x10 10.2 us: shift(): lax.ppermute(value, 'tp', [(n, (n + distance) % 8) for n in range(8)])]
    all_to_all x7 -> x6, starting transfers between devices: 38.9 us -> 38.9 us  [exchange(): return lax.all_to_all(value, axis, 0, 0, tiled=True)]
  transfers between devices with their start and end apart: 14 -> 17, of which waited for: 6 -> 7; matrix products, arithmetic and copies ran while one was open for 4% -> 4% of each run, Pallas kernels for 29% -> 29%
where the time goes in v2:
time: 129 us; the launch traced here: 127 us
  starting transfers between devices  49.2 us (38%)
  Pallas kernels  38.3 us (30%)
  waiting for transfers between devices  32.9 us (26%)
  other arithmetic  2.52 us (2%)
  local copies, waits for them, and re-layouts  1.96 us (2%)
  matrix products  1.47 us (1%)
    all_to_all x6, starting transfers between devices, exchange(): return lax.all_to_all(value, axis, 0, 0, tiled=True)  38.9 us
    all_to_all x6, waiting for transfers between devices, exchange(): return lax.all_to_all(value, axis, 0, 0, tiled=True)  30.4 us
    pallas_call x3, Pallas kernels, copy_cache(): pl.pallas_call(kernel, out_shape=jax.ShapeDtypeStruct(cache.shape, cache....  21.7 us
    ppermute x10, starting transfers between devices, shift(): lax.ppermute(value, 'tp', [(n, (n + distance) % 8) for n in range(8)])  10.2 us
    pallas_call x1, Pallas kernels, attend(): pl.pallas_call(attend_kernel, out_shape=(jax.ShapeDtypeStruct((16, 32, 12...  7.07 us
  transfers between devices with their start and end apart: 17, of which 7 were waited for; matrix products, arithmetic and copies ran while one was open for 4% of the time, Pallas kernels for 29%

profile of v2, /device:TPU:0, one launch (start us, length us, event | category | flops | bytes accessed | tf_op | source)
XLA Modules:
  0.0 127.2 jit_solution(10147402923380680840)
XLA Ops:
  0.7 1.8 %shard_map.149 = bf16[128,16,128]{2,1,0:T(8,128)(2,1)} custom-call(bf16[16,384]{1,0:T(8,128)(2,1)} %bitcast.44, bf16[16,512]{1,0:T(8,128)(2,1)} %q_ref.1, bf16[16,288]{1,0:T(8,128)(2,1)} %k_ref.1, bf16[1,16]{1,0:T(2,128)(2,1)} %bitcast.45), custom_call_target="tpu_custom_call" | custom-call | flops 100000000 | bytes 1000000 | tf_op jit(solution)/shard_map/pallas_call | solution.py:108
  2.6 11.3 %all-to-all-start = ((bf16[128,16,128]{2,1,0:T(8,128)(2,1)}), bf16[128,16,128]{2,1,0:T(8,128)(2,1)S(1)}, u32[]{:S(2)}, u32[]{:S(2)}) async-start(bf16[128,16,128]{2,1,0:T(8,128)(2,1)} %shard_map.149), calls=%async_computation | async-start | bytes 1048576 | tf_op jit(solution)/shard_map/all_to_all | solution.py:625
  13.9 0.7 bitcast_convert_fusion.gq_ref
  14.5 0.8 copy.21
  18.0 9.3 %all-to-all-done = bf16[128,16,128]{2,1,0:T(8,128)(2,1)S(1)} async-done(((bf16[128,16,128]{2,1,0:T(8,128)(2,1)}), bf16[128,16,128]{2,1,0:T(8,128)(2,1)S(1)}, u32[]{:S(2)}, u32[]{:S(2)}) %all-to-all-start) | async-done | bytes 524320 | tf_op jit(solution)/shard_map/all_to_all | solution.py:625
  27.3 1.4 %shard_map.150 = f32[8,24,128]{2,1,0:T(8,128)} custom-call(bf16[2048,128]{1,0:T(8,128)(2,1)S(1)} %bitcast.31), custom_call_target="tpu_custom_call" | custom-call | flops 67108864 | bytes 524288 | tf_op jit(solution)/shard_map/pallas_call | solution.py:127
  28.7 3.4 %all-to-all-start.1 = ((f32[8,24,128]{2,1,0:T(8,128)}), f32[8,24,128]{2,1,0:T(8,128)S(1)}, u32[]{:S(2)}, u32[]{:S(2)}) async-start(f32[8,24,128]{2,1,0:T(8,128)} %shard_map.150), calls=%async_computation.1 | async-start | bytes 196608 | tf_op jit(solution)/shard_map/all_to_all | solution.py:625
  32.7 5.1 %all-to-all-done.1.y_ref = f32[8,24,128]{2,1,0:T(8,128)S(1)} async-done(((f32[8,24,128]{2,1,0:T(8,128)}), f32[8,24,128]{2,1,0:T(8,128)S(1)}, u32[]{:S(2)}, u32[]{:S(2)}) %all-to-all-start.1) | async-done | bytes 98336 | tf_op jit(solution)/shard_map/all_to_all | solution.py:625
  37.8 1.1 copy-done
  38.8 1.5 %queries.1 = bf16[128,24,128]{2,1,0:T(8,128)(2,1)} custom-call(s32[1]{0:T(128)} %bitcast.t_ref, f32[8,24,128]{2,1,0:T(8,128)S(1)} %all-to-all-done.1.y_ref, f32[4,128]{1,0:T(4,128)S(1)} %bitcast_convert_fusion.gq_ref, f32[2,128]{1,0:T(2,128)S(1)} %bitcast_convert_fusion.2.gk_ref, f32[24,128]{1,0:T(8,128)S(1)} %get-tuple-element.16.cos_ref, ...), custom_call_target="tpu_custom_call" | custom-call | flops 14155776 | bytes 786432 | tf_op jit(solution)/shard_map/queries/pallas_call | solution.py:205
  40.3 4.6 %all-to-all-start.2 = ((bf16[128,24,128]{2,1,0:T(8,128)(2,1)}), bf16[128,24,128]{2,1,0:T(8,128)(2,1)S(1)}, u32[]{:S(2)}, u32[]{:S(2)}) async-start(bf16[128,24,128]{2,1,0:T(8,128)(2,1)} %queries.1), calls=%async_computation.2 | async-start | bytes 1572864 | tf_op jit(solution)/shard_map/all_to_all | solution.py:625
  45.1 5.3 %copy_cache.3.refs_1_ = bf16[24,288,2048]{2,1,0:T(8,128)(2,1)} custom-call(bf16[24,288,2048]{2,1,0:T(8,128)(2,1)} %bitcast.35), custom_call_target="tpu_custom_call" | custom-call | flops 4499999744 | bytes 11796480 | tf_op jit(solution)/shard_map/copy_cache/pallas_call | solution.py:515
  50.4 10.8 %all-to-all-done.2.z_ref = bf16[128,24,128]{2,1,0:T(8,128)(2,1)S(1)} async-done(((bf16[128,24,128]{2,1,0:T(8,128)(2,1)}), bf16[128,24,128]{2,1,0:T(8,128)(2,1)S(1)}, u32[]{:S(2)}, u32[]{:S(2)}) %all-to-all-start.2) | async-done | bytes 786464 | tf_op jit(solution)/shard_map/all_to_all | solution.py:625
  61.2 7.1 %attend.1 = (bf16[16,32,128]{2,1,0:T(8,128)(2,1)}, bf16[24,16,384]{2,1,0:T(8,128)(2,1)S(1)}) custom-call(s32[25]{0:T(128)S(1)} %pad_add_fusion.n_ref, bf16[128,24,128]{2,1,0:T(8,128)(2,1)S(1)} %all-to-all-done.2.z_ref, bf16[24,288,2048]{2,1,0:T(8,128)(2,1)} %bitcast.36, f32[3,128,128]{2,1,0:T(8,128)S(1)} %broadcast_bitcast_fusion.anc_ref, ...), custom_call_target="tpu_custom_call" | custom-call | flops 1711276032 | bytes 3538944 | tf_op jit(solution)/shard_map/attend/pallas_call | solution.py:360
  68.3 3.5 %all-to-all-start.3 = ((bf16[16,32,128]{2,1,0:T(8,128)(2,1)}), bf16[16,32,128]{2,1,0:T(8,128)(2,1)S(1)}, u32[]{:S(2)}, u32[]{:S(2)}) async-start(bf16[16,32,128]{2,1,0:T(8,128)(2,1)} %get-tuple-element.6), calls=%async_computation.3 | async-start | bytes 262144 | tf_op jit(solution)/shard_map/all_to_all | solution.py:625
  71.9 3.8 %copy_cache.4.refs_1_ = bf16[24,288,2048]{2,1,0:T(8,128)(2,1)} custom-call(bf16[24,288,2048]{2,1,0:T(8,128)(2,1)} %bitcast.37, bf16[24,288,2048]{2,1,0:T(8,128)(2,1)} %copy_cache.3.refs_1_), custom_call_target="tpu_custom_call", output_to_operand_aliasing={{}: (1, {})} | custom-call | flops 3600000000 | bytes 9437184 | tf_op jit(solution)/shard_map/copy_cache/pallas_call | solution.py:515
  75.7 1.1 collective-permute-start.3
  76.8 1.5 %collective-permute-start.2 = (bf16[2,128,128]{2,1,0:T(8,128)(2,1)S(1)}, bf16[2,128,128]{2,1,0:T(8,128)(2,1)S(1)}, u32[]{:S(2)}, u32[]{:S(2)}) collective-permute-start(bf16[2,128,128]{2,1,0:T(8,128)(2,1)S(1)} %pad_maximum_fusion.refs_0_), channel_id=1, source_target_pairs={{0,4},{1,5},{2,6},{3,7},{4,0},{5,1},{6,2},{7,3},{8,12},{9,13},{10,... | collective-permute-start | bytes 196616 | tf_op jit(solution)/shard_map/ppermute | solution.py:687
  78.3 1.5 %all-to-all-done.3.v_ref = bf16[16,32,128]{2,1,0:T(8,128)(2,1)S(1)} async-done(((bf16[16,32,128]{2,1,0:T(8,128)(2,1)}), bf16[16,32,128]{2,1,0:T(8,128)(2,1)S(1)}, u32[]{:S(2)}, u32[]{:S(2)}) %all-to-all-start.3) | async-done | bytes 131104 | tf_op jit(solution)/shard_map/all_to_all | solution.py:625
  79.8 0.9 shard_map.151
  80.7 5.7 %all-to-all-start.4 = ((bf16[16,24,128]{2,1,0:T(8,128)(2,1)}), bf16[16,24,128]{2,1,0:T(8,128)(2,1)S(1)}, u32[]{:S(2)}, u32[]{:S(2)}) async-start(bf16[16,24,128]{2,1,0:T(8,128)(2,1)} %shard_map.151), calls=%async_computation.4 | async-start | bytes 196608 | tf_op jit(solution)/shard_map/all_to_all | solution.py:625
  86.4 12.6 %copy_cache.5.old_ref = bf16[24,288,2048]{2,1,0:T(8,128)(2,1)} custom-call(bf16[24,288,2048]{2,1,0:T(8,128)(2,1)} %bitcast.38, bf16[24,288,2048]{2,1,0:T(8,128)(2,1)} %copy_cache.4.refs_1_), custom_call_target="tpu_custom_call", output_to_operand_aliasing={{}: (1, {})} | custom-call | flops 13500000256 | bytes 35389440 | tf_op jit(solution)/shard_map/copy_cache/pallas_call | solution.py:515
  99.1 1.0 mix.1
  100.7 2.7 %collective-permute-start.9 = (f32[48,128]{1,0:T(8,128)S(1)}, f32[48,128]{1,0:T(8,128)S(1)}, u32[]{:S(2)}, u32[]{:S(2)}) collective-permute-start(f32[48,128]{1,0:T(8,128)S(1)} %get-tuple-element.8.refs_0_), channel_id=1, source_target_pairs={{0,6},{1,7},{2,0},{3,1},{4,2},{5,3},{6,4},{7,5},{8,14},{9,15},{10,... | collective-permute-start | bytes 73736 | tf_op jit(solution)/shard_map/ppermute | solution.py:687
  103.4 0.7 collective-permute-start.8
  104.1 2.6 %collective-permute-start.7 = (f32[48,128]{1,0:T(8,128)S(1)}, f32[48,128]{1,0:T(8,128)S(1)}, u32[]{:S(2)}, u32[]{:S(2)}) collective-permute-start(f32[48,128]{1,0:T(8,128)S(1)} %get-tuple-element.8.refs_0_), channel_id=1, source_target_pairs={{0,4},{1,5},{2,6},{3,7},{4,0},{5,1},{6,2},{7,3},{8,12},{9,13},{10,... | collective-permute-start | bytes 73736 | tf_op jit(solution)/shard_map/ppermute | solution.py:687
  106.7 10.5 %all-to-all-start.5 = ((f32[128,1,128]{2,1,0:T(1,128)}), f32[128,1,128]{2,1,0:T(1,128)S(1)}, u32[]{:S(2)}, u32[]{:S(2)}) async-start(f32[128,1,128]{2,1,0:T(1,128)} %get-tuple-element.7), calls=%async_computation.5 | async-start | bytes 131072 | tf_op jit(solution)/shard_map/all_to_all | solution.py:625
  117.2 1.0 collective-permute-start.5
  118.2 2.1 %place.1 = bf16[24,288,2048]{2,1,0:T(8,128)(2,1)} custom-call(s32[25]{0:T(128)S(1)} %pad_add_fusion.n_ref, bf16[24,288,2048]{2,1,0:T(8,128)(2,1)} %bitcast.39, bf16[24,16,384]{2,1,0:T(8,128)(2,1)S(1)} %get-tuple-element.9.fresh_ref, bf16[24,288,2048]{2,1,0:T(8,128)(2,1)} %copy_cache.5.old_ref), custom_call_target="tpu_custom_call", output_to_operand_aliasing={{}: (3, {})} | custom-call | flops 1000000000 | bytes 2000000 | tf_op jit(solution)/shard_map/place/pallas_call | solution.py:593
  120.3 2.0 %collective-permute-done.5.refs_2_ = f32[48,128]{1,0:T(8,128)S(1)} collective-permute-done((f32[48,128]{1,0:T(8,128)S(1)}, f32[48,128]{1,0:T(8,128)S(1)}, u32[]{:S(2)}, u32[]{:S(2)}) %collective-permute-start.5) | collective-permute-done | bytes 24608 | tf_op jit(solution)/shard_map/ppermute | solution.py:687
  122.8 3.7 %all-to-all-done.5 = f32[128,1,128]{2,1,0:T(1,128)S(1)} async-done(((f32[128,1,128]{2,1,0:T(1,128)}), f32[128,1,128]{2,1,0:T(1,128)S(1)}, u32[]{:S(2)}, u32[]{:S(2)}) %all-to-all-start.5) | async-done | bytes 65568 | tf_op jit(solution)/shard_map/all_to_all | solution.py:625
  126.4 0.8 finish.1
  (42 shorter events, 4.6 us)
Async XLA Ops:
  0.6 75.1 %collective-permute-start = (bf16[128,128]{1,0:T(8,128)(2,1)}, bf16[128,128]{1,0:T(8,128)(2,1)S(1)}, u32[]{:S(2)}, u32[]{:S(2)}) collective-permute-start(bf16[128,128]{1,0:T(8,128)(2,1)} %param.26), channel_id=1, source_target_pairs={{0,1},{1,0},{2,3},{3,2},{4,5},{5,4},{6,7},{7,6},{8,9},{9,8},{10,11... | collective-permute-start | bytes 98312 | tf_op jit(solution)/shard_map/ppermute | solution.py:689
  2.6 24.8 %all-to-all-start = ((bf16[128,16,128]{2,1,0:T(8,128)(2,1)}), bf16[128,16,128]{2,1,0:T(8,128)(2,1)S(1)}, u32[]{:S(2)}, u32[]{:S(2)}) async-start(bf16[128,16,128]{2,1,0:T(8,128)(2,1)} %shard_map.149), calls=%async_computation | async-start | bytes 1048576 | tf_op jit(solution)/shard_map/all_to_all | solution.py:625
  28.7 9.1 %all-to-all-start.1 = ((f32[8,24,128]{2,1,0:T(8,128)}), f32[8,24,128]{2,1,0:T(8,128)S(1)}, u32[]{:S(2)}, u32[]{:S(2)}) async-start(f32[8,24,128]{2,1,0:T(8,128)} %shard_map.150), calls=%async_computation.1 | async-start | bytes 196608 | tf_op jit(solution)/shard_map/all_to_all | solution.py:625
  37.8 1.1 copy-start
  40.3 20.9 %all-to-all-start.2 = ((bf16[128,24,128]{2,1,0:T(8,128)(2,1)}), bf16[128,24,128]{2,1,0:T(8,128)(2,1)S(1)}, u32[]{:S(2)}, u32[]{:S(2)}) async-start(bf16[128,24,128]{2,1,0:T(8,128)(2,1)} %queries.1), calls=%async_computation.2 | async-start | bytes 1572864 | tf_op jit(solution)/shard_map/all_to_all | solution.py:625
  45.1 16.1 %copy-start.1 = (bf16[16,256,64]{1,2,0:T(8,128)(2,1)S(1)}, bf16[16,256,64]{1,2,0:T(8,128)(2,1)}, u32[]{:S(2)}) copy-start(bf16[16,256,64]{1,2,0:T(8,128)(2,1)} %param.25) | copy-start | bytes 1572868
  68.3 11.5 %all-to-all-start.3 = ((bf16[16,32,128]{2,1,0:T(8,128)(2,1)}), bf16[16,32,128]{2,1,0:T(8,128)(2,1)S(1)}, u32[]{:S(2)}, u32[]{:S(2)}) async-start(bf16[16,32,128]{2,1,0:T(8,128)(2,1)} %get-tuple-element.6), calls=%async_computation.3 | async-start | bytes 262144 | tf_op jit(solution)/shard_map/all_to_all | solution.py:625
  71.8 3.9 %copy-start.2 = (bf16[128,128]{1,0:T(8,128)(2,1)S(1)}, bf16[128,128]{1,0:T(8,128)(2,1)}, u32[]{:S(2)}) copy-start(bf16[128,128]{1,0:T(8,128)(2,1)} %param.26) | copy-start | bytes 98308
  75.7 23.3 %collective-permute-start.3 = (bf16[2,128,128]{2,1,0:T(8,128)(2,1)S(1)}, bf16[2,128,128]{2,1,0:T(8,128)(2,1)S(1)}, u32[]{:S(2)}, u32[]{:S(2)}) collective-permute-start(bf16[2,128,128]{2,1,0:T(8,128)(2,1)S(1)} %pad_maximum_fusion.refs_0_), channel_id=1, source_target_pairs={{0,6},{1,7},{2,0},{3,1},{4,2},{5,3},{6,4},{7,5},{8,14},{9,15},{10,... | collective-permute-start | bytes 196616 | tf_op jit(solution)/shard_map/ppermute | solution.py:687
  76.8 22.3 %collective-permute-start.2 = (bf16[2,128,128]{2,1,0:T(8,128)(2,1)S(1)}, bf16[2,128,128]{2,1,0:T(8,128)(2,1)S(1)}, u32[]{:S(2)}, u32[]{:S(2)}) collective-permute-start(bf16[2,128,128]{2,1,0:T(8,128)(2,1)S(1)} %pad_maximum_fusion.refs_0_), channel_id=1, source_target_pairs={{0,4},{1,5},{2,6},{3,7},{4,0},{5,1},{6,2},{7,3},{8,12},{9,13},{10,... | collective-permute-start | bytes 196616 | tf_op jit(solution)/shard_map/ppermute | solution.py:687
  78.3 20.8 %collective-permute-start.1 = (bf16[2,128,128]{2,1,0:T(8,128)(2,1)S(1)}, bf16[2,128,128]{2,1,0:T(8,128)(2,1)S(1)}, u32[]{:S(2)}, u32[]{:S(2)}) collective-permute-start(bf16[2,128,128]{2,1,0:T(8,128)(2,1)S(1)} %pad_maximum_fusion.refs_0_), channel_id=1, source_target_pairs={{0,2},{1,3},{2,4},{3,5},{4,6},{5,7},{6,0},{7,1},{8,10},{9,11},{10,... | collective-permute-start | bytes 196616 | tf_op jit(solution)/shard_map/ppermute | solution.py:687
  80.7 18.3 %all-to-all-start.4 = ((bf16[16,24,128]{2,1,0:T(8,128)(2,1)}), bf16[16,24,128]{2,1,0:T(8,128)(2,1)S(1)}, u32[]{:S(2)}, u32[]{:S(2)}) async-start(bf16[16,24,128]{2,1,0:T(8,128)(2,1)} %shard_map.151), calls=%async_computation.4 | async-start | bytes 196608 | tf_op jit(solution)/shard_map/all_to_all | solution.py:625
  86.4 17.0 %copy-start.3 = (bf16[128]{0:T(256)(128)(2,1)S(1)}, bf16[128]{0:T(256)(128)(2,1)}, u32[]{:S(2)}) copy-start(bf16[128]{0:T(256)(128)(2,1)} %param.27) | copy-start | bytes 772
  100.1 17.1 %collective-permute-start.10 = (f32[48,128]{1,0:T(8,128)S(1)}, f32[48,128]{1,0:T(8,128)S(1)}, u32[]{:S(2)}, u32[]{:S(2)}) collective-permute-start(f32[48,128]{1,0:T(8,128)S(1)} %get-tuple-element.8.refs_0_), channel_id=1, source_target_pairs={{0,7},{1,0},{2,1},{3,2},{4,3},{5,4},{6,5},{7,6},{8,15},{9,8},{10,9... | collective-permute-start | bytes 73736 | tf_op jit(solution)/shard_map/ppermute | solution.py:687
  100.7 17.6 %collective-permute-start.9 = (f32[48,128]{1,0:T(8,128)S(1)}, f32[48,128]{1,0:T(8,128)S(1)}, u32[]{:S(2)}, u32[]{:S(2)}) collective-permute-start(f32[48,128]{1,0:T(8,128)S(1)} %get-tuple-element.8.refs_0_), channel_id=1, source_target_pairs={{0,6},{1,7},{2,0},{3,1},{4,2},{5,3},{6,4},{7,5},{8,14},{9,15},{10,... | collective-permute-start | bytes 73736 | tf_op jit(solution)/shard_map/ppermute | solution.py:687
  103.4 17.0 %collective-permute-start.8 = (f32[48,128]{1,0:T(8,128)S(1)}, f32[48,128]{1,0:T(8,128)S(1)}, u32[]{:S(2)}, u32[]{:S(2)}) collective-permute-start(f32[48,128]{1,0:T(8,128)S(1)} %get-tuple-element.8.refs_0_), channel_id=1, source_target_pairs={{0,5},{1,6},{2,7},{3,0},{4,1},{5,2},{6,3},{7,4},{8,13},{9,14},{10,... | collective-permute-start | bytes 73736 | tf_op jit(solution)/shard_map/ppermute | solution.py:687
  104.1 16.3 %collective-permute-start.7 = (f32[48,128]{1,0:T(8,128)S(1)}, f32[48,128]{1,0:T(8,128)S(1)}, u32[]{:S(2)}, u32[]{:S(2)}) collective-permute-start(f32[48,128]{1,0:T(8,128)S(1)} %get-tuple-element.8.refs_0_), channel_id=1, source_target_pairs={{0,4},{1,5},{2,6},{3,7},{4,0},{5,1},{6,2},{7,3},{8,12},{9,13},{10,... | collective-permute-start | bytes 73736 | tf_op jit(solution)/shard_map/ppermute | solution.py:687
  106.7 13.6 %collective-permute-start.6 = (f32[48,128]{1,0:T(8,128)S(1)}, f32[48,128]{1,0:T(8,128)S(1)}, u32[]{:S(2)}, u32[]{:S(2)}) collective-permute-start(f32[48,128]{1,0:T(8,128)S(1)} %get-tuple-element.8.refs_0_), channel_id=1, source_target_pairs={{0,3},{1,4},{2,5},{3,6},{4,7},{5,0},{6,1},{7,2},{8,11},{9,12},{10,... | collective-permute-start | bytes 73736 | tf_op jit(solution)/shard_map/ppermute | solution.py:687
  106.7 19.7 %all-to-all-start.5 = ((f32[128,1,128]{2,1,0:T(1,128)}), f32[128,1,128]{2,1,0:T(1,128)S(1)}, u32[]{:S(2)}, u32[]{:S(2)}) async-start(f32[128,1,128]{2,1,0:T(1,128)} %get-tuple-element.7), calls=%async_computation.5 | async-start | bytes 131072 | tf_op jit(solution)/shard_map/all_to_all | solution.py:625
  117.2 5.1 %collective-permute-start.5 = (f32[48,128]{1,0:T(8,128)S(1)}, f32[48,128]{1,0:T(8,128)S(1)}, u32[]{:S(2)}, u32[]{:S(2)}) collective-permute-start(f32[48,128]{1,0:T(8,128)S(1)} %get-tuple-element.8.refs_0_), channel_id=1, source_target_pairs={{0,2},{1,3},{2,4},{3,5},{4,6},{5,7},{6,0},{7,1},{8,10},{9,11},{10,... | collective-permute-start | bytes 73736 | tf_op jit(solution)/shard_map/ppermute | solution.py:687
  118.2 4.6 %collective-permute-start.4 = (f32[48,128]{1,0:T(8,128)S(1)}, f32[48,128]{1,0:T(8,128)S(1)}, u32[]{:S(2)}, u32[]{:S(2)}) collective-permute-start(f32[48,128]{1,0:T(8,128)S(1)} %get-tuple-element.8.refs_0_), channel_id=1, source_target_pairs={{0,1},{1,2},{2,3},{3,4},{4,5},{5,6},{6,7},{7,0},{8,9},{9,10},{10,1... | collective-permute-start | bytes 73736 | tf_op jit(solution)/shard_map/ppermute | solution.py:687

commit v3 on v2

--- a/solution.py
+++ b/solution.py
@@ -3,6 +3,7 @@
 from jax import lax
 from jax.experimental import pallas as pl
 from jax.experimental.pallas import tpu as pltpu
+from jax.sharding import Mesh
 from jax.sharding import PartitionSpec as P
 
 
@@ -20,7 +21,10 @@
 EPS = 1e-06
 ROPE_BASE = 10000.0
 MASKED = -1e30
-ALL = ("kv", "tp")
+ALL = ("kv", "y", "c")
+TP = ("y", "c")
+CORES = ("kv", "c")
+PLANES = ("kv", "y")
 VMEM = pltpu.VMEM
 
 
@@ -338,22 +342,33 @@
     values(1, *second)
     values(2, *third)
     small = lanes_of((8, 128))
-    for h in range(16):
-        pieces = []
-        level = jnp.zeros((8, 128), f32)
-        for half in range(2):
-            for s in range(3):
-                rows = pl.ds((h % 2) * 128 + half * 64 + h // 2, 8, stride=8)
-                pieces.append(jnp.concatenate([part[s, a, rows, :] for a in range(2)], axis=1))
-                level = jnp.where(small // 4 == half * 3 + s, lam[s, rows, :], level)
-        out = dot_nt(jnp.concatenate(pieces, axis=0).astype(bf16), wv_ref[h])
-        out = jnp.concatenate([out[0:24], out[24:48]], axis=1)
-        first = rounded(level)
-        second = rounded(level - first)
-        third = (level - first) - second
-        level = jnp.where(small % 4 == 0, first, jnp.where(small % 4 == 1, second, third))
-        level = jnp.where(small % 4 == 3, 0.0, level)
-        o_ref[h] = jnp.concatenate([out, level], axis=0).astype(bf16)
+    short = lanes_of((24, 128))
+    for quad in range(4):
+        pieces, levels = [], []
+        for h in range(4 * quad, 4 * quad + 4):
+            level = jnp.zeros((8, 128), f32)
+            for half in range(2):
+                for s in range(3):
+                    rows = pl.ds((h % 2) * 128 + half * 64 + h // 2, 8, stride=8)
+                    pieces.append(
+                        jnp.concatenate([part[s, a, rows, :] for a in range(2)], axis=1)
+                    )
+                    level = jnp.where(small // 4 == half * 3 + s, lam[s, rows, :], level)
+            first = rounded(level)
+            second = rounded(level - first)
+            third = (level - first) - second
+            level = jnp.where(small % 4 == 0, first, jnp.where(small % 4 == 1, second, third))
+            levels.append(jnp.where(small % 4 == 3, 0.0, level))
+        weights = wv_ref[4 * quad : 4 * quad + 4].reshape(256, 256)
+        out = dot_nt(jnp.concatenate(pieces, axis=0).astype(bf16), weights)
+        for a in range(4):
+            tile = out[48 * a : 48 * a + 48, (a // 2) * 128 : (a // 2) * 128 + 128]
+            low, high = tile[0:24], tile[24:48]
+            if a % 2:
+                tile = jnp.where(short < 64, turn(low, 64), high)
+            else:
+                tile = jnp.where(short < 64, low, turn(high, 64))
+            o_ref[4 * quad + a] = jnp.concatenate([tile, levels[a]], axis=0).astype(bf16)
 
 
 def attend(numbers, z, cache, anc, wv):
@@ -397,25 +412,26 @@
 
 
 def combine(v):
-    return call(combine_kernel, jax.ShapeDtypeStruct((16, 24, 128), bf16), 1, cost(1e6, 1e5))(v)
+    return call(combine_kernel, jax.ShapeDtypeStruct((32, 24, 128), bf16), 1, cost(1e6, 1e5))(v)
 
 
 def mix_kernel(t_ref, u_ref, *refs):
     w_refs, (o_ref, s_ref) = refs[:4], refs[4:]
     lane = lanes_of((24, 128))
-    mixed = jnp.zeros((48, 128), f32)
+    mixed = jnp.zeros((96, 128), f32)
     for k in range(4):
         for b in range(2):
             p = ((t_ref[0] - 2 * k) & 7) ^ b
-            first, second = u_ref[2 * p].astype(f32), u_ref[2 * p + 1].astype(f32)
-            left = jnp.where(lane < 64, first, turn(second, 64))
-            right = jnp.where(lane < 64, turn(first, 64), second)
-            lhs = jnp.concatenate([left, right], axis=0).astype(bf16)
-            mixed = mixed + dot_nn(lhs, w_refs[k][b])
+            lhs = []
+            for c in range(2):
+                first, second = u_ref[2 * p, c].astype(f32), u_ref[2 * p + 1, c].astype(f32)
+                lhs.append(jnp.where(lane < 64, first, turn(second, 64)))
+                lhs.append(jnp.where(lane < 64, turn(first, 64), second))
+            mixed = mixed + dot_nn(jnp.concatenate(lhs, axis=0).astype(bf16), w_refs[k][b])
     o_ref[...] = mixed
     squares = jnp.broadcast_to(jnp.sum(mixed * mixed, axis=1, keepdims=True), mixed.shape)
-    row = lax.broadcasted_iota(jnp.int32, (48, 128), 0)
-    line = jnp.sum(jnp.where(row == lanes_of((48, 128)), squares, 0.0), axis=0, keepdims=True)
+    row = lax.broadcasted_iota(jnp.int32, (96, 128), 0)
+    line = jnp.sum(jnp.where(row == lanes_of((96, 128)), squares, 0.0), axis=0, keepdims=True)
     s_ref[...] = jnp.broadcast_to(line[None], s_ref.shape)
 
 
@@ -423,41 +439,43 @@
     return pl.pallas_call(
         mix_kernel,
         out_shape=(
-            jax.ShapeDtypeStruct((48, 128), f32),
-            jax.ShapeDtypeStruct((128, 1, 128), f32),
+            jax.ShapeDtypeStruct((96, 128), f32),
+            jax.ShapeDtypeStruct((64, 1, 128), f32),
         ),
         in_specs=[smem_spec()] + [vmem_spec()] * 5,
         out_specs=(vmem_spec(),) * 2,
-        cost_estimate=cost(2 * 48 * 1024 * 128, 4e5),
+        cost_estimate=cost(2 * 96 * 1024 * 128, 4e5),
         compiler_params=pltpu.CompilerParams(vmem_limit_bytes=16 << 20),
         name="mix",
     )(t, u, *w)
 
 
 def finish_kernel(t_ref, s_ref, g_ref, *refs):
-    m_refs, (o_ref, scale) = refs[:8], refs[8:]
+    m_refs, (o_ref, scale) = refs[:4], refs[4:]
     scale[...] = lax.rsqrt(jnp.sum(s_ref[...], axis=0) / D + EPS)
-    row = lax.broadcasted_iota(jnp.int32, (48, 128), 0)
-    same = row == lanes_of((48, 128))
+    row = lax.broadcasted_iota(jnp.int32, (96, 128), 0)
+    same = row == lanes_of((96, 128))
     gain = g_ref[...]
-    for k in range(8):
-        p = (t_ref[0] - k) & 7
-        inverse = scale[pl.ds(p, 1), :]
+    for k in range(4):
+        y = ((t_ref[0] >> 1) - k) & 3
+        inverse = scale[pl.ds(y, 1), :]
         column = jnp.sum(jnp.where(same, inverse, 0.0), axis=1, keepdims=True)
         out = m_refs[k][...] * column * gain
-        for s in range(3):
-            rows = jnp.concatenate([out[s * 8 : s * 8 + 8], out[24 + s * 8 : 32 + s * 8]], axis=0)
-            at = pl.multiple_of((s * 8 + p) * 16, 16)
-            o_ref[pl.ds(at, 16), :] = rows.astype(bf16)
+        for c in range(2):
+            for s in range(3):
+                at = c * 48 + s * 8
+                rows = jnp.concatenate([out[at : at + 8], out[at + 24 : at + 32]], axis=0)
+                at = pl.multiple_of((s * 8 + 2 * y + c) * 16, 16)
+                o_ref[pl.ds(at, 16), :] = rows.astype(bf16)
 
 
 def finish(t, s, g, m):
     return pl.pallas_call(
         finish_kernel,
         out_shape=jax.ShapeDtypeStruct((384, 128), bf16),
-        in_specs=[smem_spec()] + [vmem_spec()] * 10,
+        in_specs=[smem_spec()] + [vmem_spec()] * 6,
         out_specs=vmem_spec(),
-        scratch_shapes=[VMEM((8, 128), f32)],
+        scratch_shapes=[VMEM((4, 128), f32)],
         cost_estimate=cost(1e6, 4e5),
         compiler_params=pltpu.CompilerParams(vmem_limit_bytes=16 << 20),
         name="finish",
@@ -642,13 +660,13 @@
     gain_output,
 ):
     j = lax.axis_index("kv")
-    t = lax.axis_index("tp")
+    t = lax.axis_index(TP)
     mine = t[None].astype(jnp.int32)
     cache = jnp.transpose(latent_cache, (0, 2, 1))
 
     x = pack(jnp.transpose(activations), w_query_down, w_key_down, gain_input[None])
     x = exchange(x, ALL).reshape(2048, 128)
-    y = exchange(down(x), "tp")
+    y = exchange(down(x), TP)
 
     reached, depths = ancestry(parents)
     filled = lengths + accepted
@@ -676,6 +694,8 @@
         wq,
     )
     z = exchange(z, ALL)
+    other = lax.ppermute(w_out, TP, [(n, n ^ 1) for n in range(8)])
+    z, other = lax.optimization_barrier((z, other))
     sent, fresh = attend(numbers, z, cache, anc, wv)
 
     updated = None
@@ -683,16 +703,18 @@
         updated = copy_cache(cache, updated, CUTS[n], CUTS[n + 1])
     updated = place(numbers, cache, fresh, updated)
 
-    def shift(value, distance):
-        return lax.ppermute(value, "tp", [(n, (n + distance) % 8) for n in range(8)])
-
-    other = lax.ppermute(w_out, "tp", [(n, n ^ 1) for n in range(8)])
     w_here = [jnp.stack([w_out, other])]
-    w_here += [shift(w_here[0], 2 * k) for k in range(1, 4)]
-    attended = combine(exchange(sent, "kv"))
-    mixed, squares = mix(mine, exchange(attended, "kv"), w_here)
-    squares = exchange(squares, ALL).reshape(16, 8, 128)
-    mixed = [mixed] + [shift(mixed, k) for k in range(1, 8)]
+    w_here += [
+        lax.ppermute(w_here[0], "y", [(n, (n + k) % 4) for n in range(4)]) for k in range(1, 4)
+    ]
+    sent = exchange(sent, "kv")
+    attended = combine(sent)
+    attended = exchange(attended, CORES).reshape(16, 2, 24, 128)
+    mixed, squares = mix(mine, attended, w_here)
+    squares = exchange(squares, PLANES).reshape(16, 4, 128)
+    mixed = [mixed] + [
+        lax.ppermute(mixed, "y", [(n, (n + k) % 4) for n in range(4)]) for k in range(1, 4)
+    ]
     result = finish(mine, squares, gain_output.astype(f32)[None], mixed)
     return (result, jnp.transpose(updated, (0, 2, 1)))
 
@@ -701,9 +723,10 @@
 
 
 def solution(mesh):
+    split = Mesh(mesh.devices.reshape(16, 4, 2), ALL)
     return jax.shard_map(
         layer,
-        mesh=mesh,
+        mesh=split,
         in_specs=(
             P(None, ALL),
             P(None, "kv", None),
@@ -715,9 +738,9 @@
             P(ALL),
             P(),
             P(),
-            P(None, "tp", None),
+            P(None, TP, None),
             P(),
-            P("tp", "kv"),
+            P(TP, "kv"),
             P("kv"),
         ),
         out_specs=(P(None, "kv"), P(None, "kv", None)),

time: 129 us -> 127 us (0.984)
  starting transfers between devices: 49.2 us -> 44.1 us
  waiting for transfers between devices: 32.9 us -> 36.9 us
    all_to_all x6, waiting for transfers between devices: 30.4 us -> 36.9 us  [exchange(): return lax.all_to_all(value, axis, 0, 0, tiled=True)]
    ppermute x11 -> x7, starting transfers between devices: 10.3 us -> 7.73 us  [the longest x3 5.1 us: layer(): lax.ppermute(mixed, 'y', [(n, (n + k) % 4) for n in range(4)])]
    all_to_all x6, starting transfers between devices: 38.9 us -> 36.4 us  [exchange(): return lax.all_to_all(value, axis, 0, 0, tiled=True)]
    ppermute x11 -> x7, waiting for transfers between devices: 2.46 us -> 0.02 us  [the longest x3 0.01 us: layer(): lax.ppermute(w_here[0], 'y', [(n, (n + k) % 4) for n in range(4)])]
  transfers between devices with their start and end apart: 17 -> 13, of which waited for: 7 -> 5; matrix products, arithmetic and copies ran while one was open for 4% -> 4% of each run, Pallas kernels for 29% -> 23%
where the time goes in v3:
time: 127 us; the launch traced here: 126 us
  starting transfers between devices  44.1 us (35%)
  Pallas kernels  38.3 us (30%)
  waiting for transfers between devices  36.9 us (29%)
  other arithmetic  2.53 us (2%)
  local copies, waits for them, and re-layouts  1.96 us (2%)
  matrix products  1.47 us (1%)
    all_to_all x6, waiting for transfers between devices, exchange(): return lax.all_to_all(value, axis, 0, 0, tiled=True)  36.9 us
    all_to_all x6, starting transfers between devices, exchange(): return lax.all_to_all(value, axis, 0, 0, tiled=True)  36.4 us
    pallas_call x3, Pallas kernels, copy_cache(): pl.pallas_call(kernel, out_shape=jax.ShapeDtypeStruct(cache.shape, cache....  21.7 us
    pallas_call x1, Pallas kernels, attend(): pl.pallas_call(attend_kernel, out_shape=(jax.ShapeDtypeStruct((16, 32, 12...  7.05 us
    ppermute x3, starting transfers between devices, layer(): lax.ppermute(mixed, 'y', [(n, (n + k) % 4) for n in range(4)])  5.1 us
    ppermute x3, starting transfers between devices, layer(): lax.ppermute(w_here[0], 'y', [(n, (n + k) % 4) for n in range(4)])  2.55 us
  transfers between devices with their start and end apart: 13, of which 5 were waited for; matrix products, arithmetic and copies ran while one was open for 4% of the time, Pallas kernels for 23%

profile of v3, /device:TPU:0, one launch (start us, length us, event | category | flops | bytes accessed | tf_op | source)
XLA Modules:
  0.0 126.3 jit_solution(18070071777050683560)
XLA Ops:
  0.7 1.8 %shard_map.149 = bf16[128,16,128]{2,1,0:T(8,128)(2,1)} custom-call(bf16[16,384]{1,0:T(8,128)(2,1)} %bitcast.46, bf16[16,512]{1,0:T(8,128)(2,1)} %q_ref.1, bf16[16,288]{1,0:T(8,128)(2,1)} %k_ref.1, bf16[1,16]{1,0:T(2,128)(2,1)} %bitcast.47), custom_call_target="tpu_custom_call" | custom-call | flops 100000000 | bytes 1000000 | tf_op jit(solution)/shard_map/pallas_call | solution.py:112
  2.6 11.3 %all-to-all-start = ((bf16[128,16,128]{2,1,0:T(8,128)(2,1)}), bf16[128,16,128]{2,1,0:T(8,128)(2,1)S(1)}, u32[]{:S(2)}, u32[]{:S(2)}) async-start(bf16[128,16,128]{2,1,0:T(8,128)(2,1)} %shard_map.149), calls=%async_computation | async-start | bytes 1048576 | tf_op jit(solution)/shard_map/all_to_all | solution.py:643
  13.9 0.7 bitcast_convert_fusion.gq_ref
  14.6 0.8 copy.21
  17.0 0.7 add_convert_fusion
  18.1 9.3 %all-to-all-done = bf16[128,16,128]{2,1,0:T(8,128)(2,1)S(1)} async-done(((bf16[128,16,128]{2,1,0:T(8,128)(2,1)}), bf16[128,16,128]{2,1,0:T(8,128)(2,1)S(1)}, u32[]{:S(2)}, u32[]{:S(2)}) %all-to-all-start) | async-done | bytes 524320 | tf_op jit(solution)/shard_map/all_to_all | solution.py:643
  27.3 1.4 %shard_map.150 = f32[8,24,128]{2,1,0:T(8,128)} custom-call(bf16[2048,128]{1,0:T(8,128)(2,1)S(1)} %bitcast.32), custom_call_target="tpu_custom_call" | custom-call | flops 67108864 | bytes 524288 | tf_op jit(solution)/shard_map/pallas_call | solution.py:131
  28.7 3.4 %all-to-all-start.1 = ((f32[8,24,128]{2,1,0:T(8,128)}), f32[8,24,128]{2,1,0:T(8,128)S(1)}, u32[]{:S(2)}, u32[]{:S(2)}) async-start(f32[8,24,128]{2,1,0:T(8,128)} %shard_map.150), calls=%async_computation.1 | async-start | bytes 196608 | tf_op jit(solution)/shard_map/all_to_all | solution.py:643
  32.1 0.7 bitcast_convert_fusion.2.gk_ref
  32.7 5.1 %all-to-all-done.1.y_ref = f32[8,24,128]{2,1,0:T(8,128)S(1)} async-done(((f32[8,24,128]{2,1,0:T(8,128)}), f32[8,24,128]{2,1,0:T(8,128)S(1)}, u32[]{:S(2)}, u32[]{:S(2)}) %all-to-all-start.1) | async-done | bytes 98336 | tf_op jit(solution)/shard_map/all_to_all | solution.py:643
  37.8 1.1 copy-done
  38.8 1.5 %queries.1 = bf16[128,24,128]{2,1,0:T(8,128)(2,1)} custom-call(s32[1]{0:T(128)} %bitcast.t_ref, f32[8,24,128]{2,1,0:T(8,128)S(1)} %all-to-all-done.1.y_ref, f32[4,128]{1,0:T(4,128)S(1)} %bitcast_convert_fusion.gq_ref, f32[2,128]{1,0:T(2,128)S(1)} %bitcast_convert_fusion.2.gk_ref, f32[24,128]{1,0:T(8,128)S(1)} %get-tuple-element.20.cos_ref, ...), custom_call_target="tpu_custom_call" | custom-call | flops 14155776 | bytes 786432 | tf_op jit(solution)/shard_map/queries/pallas_call | solution.py:209
  40.3 4.6 %all-to-all-start.2 = ((bf16[128,24,128]{2,1,0:T(8,128)(2,1)}), bf16[128,24,128]{2,1,0:T(8,128)(2,1)S(1)}, u32[]{:S(2)}, u32[]{:S(2)}) async-start(bf16[128,24,128]{2,1,0:T(8,128)(2,1)} %queries.1), calls=%async_computation.2 | async-start | bytes 1572864 | tf_op jit(solution)/shard_map/all_to_all | solution.py:643
  44.9 5.2 %copy_cache.3.refs_1_ = bf16[24,288,2048]{2,1,0:T(8,128)(2,1)} custom-call(bf16[24,288,2048]{2,1,0:T(8,128)(2,1)} %bitcast.37), custom_call_target="tpu_custom_call" | custom-call | flops 4499999744 | bytes 11796480 | tf_op jit(solution)/shard_map/copy_cache/pallas_call | solution.py:533
  50.2 3.9 %copy_cache.4.refs_1_ = bf16[24,288,2048]{2,1,0:T(8,128)(2,1)} custom-call(bf16[24,288,2048]{2,1,0:T(8,128)(2,1)} %bitcast.38, bf16[24,288,2048]{2,1,0:T(8,128)(2,1)} %copy_cache.3.refs_1_), custom_call_target="tpu_custom_call", output_to_operand_aliasing={{}: (1, {})} | custom-call | flops 3600000000 | bytes 9437184 | tf_op jit(solution)/shard_map/copy_cache/pallas_call | solution.py:533
  54.2 7.1 %all-to-all-done.2.z_ref = bf16[128,24,128]{2,1,0:T(8,128)(2,1)S(1)} async-done(((bf16[128,24,128]{2,1,0:T(8,128)(2,1)}), bf16[128,24,128]{2,1,0:T(8,128)(2,1)S(1)}, u32[]{:S(2)}, u32[]{:S(2)}) %all-to-all-start.2) | async-done | bytes 786464 | tf_op jit(solution)/shard_map/all_to_all | solution.py:643
  61.2 7.0 %attend.1 = (bf16[16,32,128]{2,1,0:T(8,128)(2,1)}, bf16[24,16,384]{2,1,0:T(8,128)(2,1)S(1)}) custom-call(s32[25]{0:T(128)S(1)} %pad_add_fusion.n_ref, bf16[128,24,128]{2,1,0:T(8,128)(2,1)S(1)} %all-to-all-done.2.z_ref, bf16[24,288,2048]{2,1,0:T(8,128)(2,1)} %bitcast.39, f32[3,128,128]{2,1,0:T(8,128)S(1)} %broadcast_bitcast_fusion.anc_ref, ...), custom_call_target="tpu_custom_call" | custom-call | flops 1711276032 | bytes 3538944 | tf_op jit(solution)/shard_map/attend/pallas_call | solution.py:375
  68.3 3.5 %all-to-all-start.3 = ((bf16[16,32,128]{2,1,0:T(8,128)(2,1)}), bf16[16,32,128]{2,1,0:T(8,128)(2,1)S(1)}, u32[]{:S(2)}, u32[]{:S(2)}) async-start(bf16[16,32,128]{2,1,0:T(8,128)(2,1)} %get-tuple-element.9), calls=%async_computation.3 | async-start | bytes 262144 | tf_op jit(solution)/shard_map/all_to_all | solution.py:643
  71.8 12.6 %copy_cache.5.old_ref = bf16[24,288,2048]{2,1,0:T(8,128)(2,1)} custom-call(bf16[24,288,2048]{2,1,0:T(8,128)(2,1)} %bitcast.40, bf16[24,288,2048]{2,1,0:T(8,128)(2,1)} %copy_cache.4.refs_1_), custom_call_target="tpu_custom_call", output_to_operand_aliasing={{}: (1, {})} | custom-call | flops 13500000256 | bytes 35389440 | tf_op jit(solution)/shard_map/copy_cache/pallas_call | solution.py:533
  84.5 1.1 collective-permute-start.3
  85.6 1.5 %collective-permute-start.2 = (bf16[2,128,128]{2,1,0:T(8,128)(2,1)S(1)}, bf16[2,128,128]{2,1,0:T(8,128)(2,1)S(1)}, u32[]{:S(2)}, u32[]{:S(2)}) collective-permute-start(bf16[2,128,128]{2,1,0:T(8,128)(2,1)S(1)} %pad_maximum_fusion.refs_0_), channel_id=1, source_target_pairs={{0,4},{2,6},{4,0},{6,2},{1,5},{3,7},{5,1},{7,3},{8,12},{10,14},{12... | collective-permute-start | bytes 196616 | tf_op jit(solution)/shard_map/ppermute | solution.py:708
  87.1 1.0 shard_map.151
  88.0 7.4 %all-to-all-start.4 = ((bf16[32,24,128]{2,1,0:T(8,128)(2,1)}), bf16[32,24,128]{2,1,0:T(8,128)(2,1)S(1)}, u32[]{:S(2)}, u32[]{:S(2)}) async-start(bf16[32,24,128]{2,1,0:T(8,128)(2,1)} %shard_map.151), calls=%async_computation.4 | async-start | bytes 393216 | tf_op jit(solution)/shard_map/all_to_all | solution.py:643
  95.5 8.1 %all-to-all-done.4 = bf16[32,24,128]{2,1,0:T(8,128)(2,1)S(1)} async-done(((bf16[32,24,128]{2,1,0:T(8,128)(2,1)}), bf16[32,24,128]{2,1,0:T(8,128)(2,1)S(1)}, u32[]{:S(2)}, u32[]{:S(2)}) %all-to-all-start.4) | async-done | bytes 196640 | tf_op jit(solution)/shard_map/all_to_all | solution.py:643
  103.6 1.0 mix.1
  104.6 3.2 %collective-permute-start.6 = (f32[96,128]{1,0:T(8,128)S(1)}, f32[96,128]{1,0:T(8,128)S(1)}, u32[]{:S(2)}, u32[]{:S(2)}) collective-permute-start(f32[96,128]{1,0:T(8,128)S(1)} %get-tuple-element.12.refs_0_), channel_id=1, source_target_pairs={{0,6},{2,0},{4,2},{6,4},{1,7},{3,1},{5,3},{7,5},{8,14},{10,8},{12,... | collective-permute-start | bytes 147464 | tf_op jit(solution)/shard_map/ppermute | solution.py:716
  107.9 0.9 collective-permute-start.5
  108.8 1.0 collective-permute-start.4
  109.7 6.2 %all-to-all-start.5 = ((f32[64,1,128]{2,1,0:T(1,128)}), f32[64,1,128]{2,1,0:T(1,128)S(1)}, u32[]{:S(2)}, u32[]{:S(2)}) async-start(f32[64,1,128]{2,1,0:T(1,128)} %get-tuple-element.11), calls=%async_computation.5 | async-start | bytes 65536 | tf_op jit(solution)/shard_map/all_to_all | solution.py:643
  115.9 2.1 %place.1 = bf16[24,288,2048]{2,1,0:T(8,128)(2,1)} custom-call(s32[25]{0:T(128)S(1)} %pad_add_fusion.n_ref, bf16[24,288,2048]{2,1,0:T(8,128)(2,1)} %bitcast.41, bf16[24,16,384]{2,1,0:T(8,128)(2,1)S(1)} %get-tuple-element.13.fresh_ref, bf16[24,288,2048]{2,1,0:T(8,128)(2,1)} %copy_cache.5.old_ref), custom_call_target="tpu_custom_call", output_to_operand_aliasing={{}: (3, {})} | custom-call | flops 1000000000 | bytes 2000000 | tf_op jit(solution)/shard_map/place/pallas_call | solution.py:611
  118.0 7.4 %all-to-all-done.5 = f32[64,1,128]{2,1,0:T(1,128)S(1)} async-done(((f32[64,1,128]{2,1,0:T(1,128)}), f32[64,1,128]{2,1,0:T(1,128)S(1)}, u32[]{:S(2)}, u32[]{:S(2)}) %all-to-all-start.5) | async-done | bytes 32800 | tf_op jit(solution)/shard_map/all_to_all | solution.py:643
  125.4 0.8 finish.1
  (34 shorter events, 2.2 us)
Async XLA Ops:
  0.6 53.5 %collective-permute-start = (bf16[128,128]{1,0:T(8,128)(2,1)}, bf16[128,128]{1,0:T(8,128)(2,1)S(1)}, u32[]{:S(2)}, u32[]{:S(2)}) collective-permute-start(bf16[128,128]{1,0:T(8,128)(2,1)} %param.26), channel_id=1, source_target_pairs={{0,1},{1,0},{2,3},{3,2},{4,5},{5,4},{6,7},{7,6},{8,9},{9,8},{10,11... | collective-permute-start | bytes 98312 | tf_op jit(solution)/shard_map/ppermute | solution.py:697
  2.6 24.8 %all-to-all-start = ((bf16[128,16,128]{2,1,0:T(8,128)(2,1)}), bf16[128,16,128]{2,1,0:T(8,128)(2,1)S(1)}, u32[]{:S(2)}, u32[]{:S(2)}) async-start(bf16[128,16,128]{2,1,0:T(8,128)(2,1)} %shard_map.149), calls=%async_computation | async-start | bytes 1048576 | tf_op jit(solution)/shard_map/all_to_all | solution.py:643
  28.7 9.1 %all-to-all-start.1 = ((f32[8,24,128]{2,1,0:T(8,128)}), f32[8,24,128]{2,1,0:T(8,128)S(1)}, u32[]{:S(2)}, u32[]{:S(2)}) async-start(f32[8,24,128]{2,1,0:T(8,128)} %shard_map.150), calls=%async_computation.1 | async-start | bytes 196608 | tf_op jit(solution)/shard_map/all_to_all | solution.py:643
  37.8 1.1 copy-start
  40.3 20.9 %all-to-all-start.2 = ((bf16[128,24,128]{2,1,0:T(8,128)(2,1)}), bf16[128,24,128]{2,1,0:T(8,128)(2,1)S(1)}, u32[]{:S(2)}, u32[]{:S(2)}) async-start(bf16[128,24,128]{2,1,0:T(8,128)(2,1)} %queries.1), calls=%async_computation.2 | async-start | bytes 1572864 | tf_op jit(solution)/shard_map/all_to_all | solution.py:643
  50.2 11.0 %copy-start.1 = (bf16[16,256,64]{1,2,0:T(8,128)(2,1)S(1)}, bf16[16,256,64]{1,2,0:T(8,128)(2,1)}, u32[]{:S(2)}) copy-start(bf16[16,256,64]{1,2,0:T(8,128)(2,1)} %param.25) | copy-start | bytes 1572868
  68.3 18.8 %all-to-all-start.3 = ((bf16[16,32,128]{2,1,0:T(8,128)(2,1)}), bf16[16,32,128]{2,1,0:T(8,128)(2,1)S(1)}, u32[]{:S(2)}, u32[]{:S(2)}) async-start(bf16[16,32,128]{2,1,0:T(8,128)(2,1)} %get-tuple-element.9), calls=%async_computation.3 | async-start | bytes 262144 | tf_op jit(solution)/shard_map/all_to_all | solution.py:643
  71.8 12.7 %copy-start.2 = (bf16[128,128]{1,0:T(8,128)(2,1)S(1)}, bf16[128,128]{1,0:T(8,128)(2,1)}, u32[]{:S(2)}) copy-start(bf16[128,128]{1,0:T(8,128)(2,1)} %param.26) | copy-start | bytes 98308
  71.8 23.7 %copy-start.3 = (bf16[128]{0:T(256)(128)(2,1)S(1)}, bf16[128]{0:T(256)(128)(2,1)}, u32[]{:S(2)}) copy-start(bf16[128]{0:T(256)(128)(2,1)} %param.27) | copy-start | bytes 772
  84.5 11.0 %collective-permute-start.3 = (bf16[2,128,128]{2,1,0:T(8,128)(2,1)S(1)}, bf16[2,128,128]{2,1,0:T(8,128)(2,1)S(1)}, u32[]{:S(2)}, u32[]{:S(2)}) collective-permute-start(bf16[2,128,128]{2,1,0:T(8,128)(2,1)S(1)} %pad_maximum_fusion.refs_0_), channel_id=1, source_target_pairs={{0,6},{2,0},{4,2},{6,4},{1,7},{3,1},{5,3},{7,5},{8,14},{10,8},{12,... | collective-permute-start | bytes 196616 | tf_op jit(solution)/shard_map/ppermute | solution.py:708
  85.6 10.0 %collective-permute-start.2 = (bf16[2,128,128]{2,1,0:T(8,128)(2,1)S(1)}, bf16[2,128,128]{2,1,0:T(8,128)(2,1)S(1)}, u32[]{:S(2)}, u32[]{:S(2)}) collective-permute-start(bf16[2,128,128]{2,1,0:T(8,128)(2,1)S(1)} %pad_maximum_fusion.refs_0_), channel_id=1, source_target_pairs={{0,4},{2,6},{4,0},{6,2},{1,5},{3,7},{5,1},{7,3},{8,12},{10,14},{12... | collective-permute-start | bytes 196616 | tf_op jit(solution)/shard_map/ppermute | solution.py:708
  87.0 8.5 %collective-permute-start.1 = (bf16[2,128,128]{2,1,0:T(8,128)(2,1)S(1)}, bf16[2,128,128]{2,1,0:T(8,128)(2,1)S(1)}, u32[]{:S(2)}, u32[]{:S(2)}) collective-permute-start(bf16[2,128,128]{2,1,0:T(8,128)(2,1)S(1)} %pad_maximum_fusion.refs_0_), channel_id=1, source_target_pairs={{0,2},{2,4},{4,6},{6,0},{1,3},{3,5},{5,7},{7,1},{8,10},{10,12},{12... | collective-permute-start | bytes 196616 | tf_op jit(solution)/shard_map/ppermute | solution.py:708
  88.0 15.6 %all-to-all-start.4 = ((bf16[32,24,128]{2,1,0:T(8,128)(2,1)}), bf16[32,24,128]{2,1,0:T(8,128)(2,1)S(1)}, u32[]{:S(2)}, u32[]{:S(2)}) async-start(bf16[32,24,128]{2,1,0:T(8,128)(2,1)} %shard_map.151), calls=%async_computation.4 | async-start | bytes 393216 | tf_op jit(solution)/shard_map/all_to_all | solution.py:643
  104.6 20.8 %collective-permute-start.6 = (f32[96,128]{1,0:T(8,128)S(1)}, f32[96,128]{1,0:T(8,128)S(1)}, u32[]{:S(2)}, u32[]{:S(2)}) collective-permute-start(f32[96,128]{1,0:T(8,128)S(1)} %get-tuple-element.12.refs_0_), channel_id=1, source_target_pairs={{0,6},{2,0},{4,2},{6,4},{1,7},{3,1},{5,3},{7,5},{8,14},{10,8},{12,... | collective-permute-start | bytes 147464 | tf_op jit(solution)/shard_map/ppermute | solution.py:716
  107.9 17.6 %collective-permute-start.5 = (f32[96,128]{1,0:T(8,128)S(1)}, f32[96,128]{1,0:T(8,128)S(1)}, u32[]{:S(2)}, u32[]{:S(2)}) collective-permute-start(f32[96,128]{1,0:T(8,128)S(1)} %get-tuple-element.12.refs_0_), channel_id=1, source_target_pairs={{0,4},{2,6},{4,0},{6,2},{1,5},{3,7},{5,1},{7,3},{8,12},{10,14},{12... | collective-permute-start | bytes 147464 | tf_op jit(solution)/shard_map/ppermute | solution.py:716
  108.8 16.7 %collective-permute-start.4 = (f32[96,128]{1,0:T(8,128)S(1)}, f32[96,128]{1,0:T(8,128)S(1)}, u32[]{:S(2)}, u32[]{:S(2)}) collective-permute-start(f32[96,128]{1,0:T(8,128)S(1)} %get-tuple-element.12.refs_0_), channel_id=1, source_target_pairs={{0,2},{2,4},{4,6},{6,0},{1,3},{3,5},{5,7},{7,1},{8,10},{10,12},{12... | collective-permute-start | bytes 147464 | tf_op jit(solution)/shard_map/ppermute | solution.py:716
  109.7 15.7 %all-to-all-start.5 = ((f32[64,1,128]{2,1,0:T(1,128)}), f32[64,1,128]{2,1,0:T(1,128)S(1)}, u32[]{:S(2)}, u32[]{:S(2)}) async-start(f32[64,1,128]{2,1,0:T(1,128)} %get-tuple-element.11), calls=%async_computation.5 | async-start | bytes 65536 | tf_op jit(solution)/shard_map/all_to_all | solution.py:643

commit v4 on v3

--- a/solution.py
+++ b/solution.py
@@ -222,30 +222,47 @@
 LOG2E = 1.4426950408889634
 
 
+def keys_kernel(n_ref, cache_ref, o_ref, sems):
+    mine = n_ref[24]
+
+    def fetch(s):
+        return pltpu.make_async_copy(cache_ref.at[s * 8 + mine], o_ref.at[s], sems.at[s])
+
+    for s in range(3):
+        fetch(s).start()
+    for s in range(3):
+        fetch(s).wait()
+
+
+def own_keys(numbers, cache):
+    return pl.pallas_call(
+        keys_kernel,
+        out_shape=jax.ShapeDtypeStruct((3, LINES, SPAN), bf16),
+        in_specs=[smem_spec(), any_spec()],
+        out_specs=vmem_spec(),
+        scratch_shapes=[pltpu.SemaphoreType.DMA((3,))],
+        cost_estimate=cost(1e8, 3 * LINES * SPAN * 4),
+        compiler_params=pltpu.CompilerParams(vmem_limit_bytes=40 << 20),
+        name="own_keys",
+    )(numbers, cache)
+
+
 def attend_kernel(
     n_ref,
     z_ref,
-    cache_ref,
+    keys,
     anc_ref,
     wv_ref,
     o_ref,
     fresh_ref,
-    keys,
     wide,
     lines,
     part,
     lam,
     score,
     prob,
-    sems,
 ):
     mine = n_ref[24]
-
-    def fetch(s):
-        return pltpu.make_async_copy(cache_ref.at[s * 8 + mine], keys.at[s], sems.at[s])
-
-    for s in range(3):
-        fetch(s).start()
     wide[...] = z_ref[...].astype(f32)
     lane = lanes_of((128, 128))
     packed = [wide[:, 18 + r, :] for r in range(3)]
@@ -332,10 +349,7 @@
         level = jnp.where(total > 0.0, top + jnp.log2(jnp.maximum(total, 1.0)), MASKED)
         lam[s] = jnp.broadcast_to(level, (256, 128))
 
-    fetch(0).wait()
     first = scores(0)
-    fetch(1).wait()
-    fetch(2).wait()
     second = scores(1)
     values(0, *first)
     third = scores(2)
@@ -371,29 +385,27 @@
             o_ref[4 * quad + a] = jnp.concatenate([tile, levels[a]], axis=0).astype(bf16)
 
 
-def attend(numbers, z, cache, anc, wv):
+def attend(numbers, z, keys, anc, wv):
     return pl.pallas_call(
         attend_kernel,
         out_shape=(
             jax.ShapeDtypeStruct((16, 32, 128), bf16),
             jax.ShapeDtypeStruct((24, 16, 384), bf16),
         ),
-        in_specs=[smem_spec(), vmem_spec(), any_spec(), vmem_spec(), vmem_spec()],
+        in_specs=[smem_spec()] + [vmem_spec()] * 4,
         out_specs=(vmem_spec(), vmem_spec()),
         scratch_shapes=[
-            VMEM((3, LINES, SPAN), bf16),
             VMEM((128, 24, 128), f32),
             VMEM((3, 3, 128, 128), f32),
             VMEM((3, 2, 256, 128), f32),
             VMEM((3, 256, 128), f32),
             VMEM((3, 256, SPAN), f32),
             VMEM((3, 256, SPAN), bf16),
-            pltpu.SemaphoreType.DMA((3,)),
         ],
         cost_estimate=cost(3 * 2 * 256 * 2048 * 544, 3 * LINES * SPAN * 2),
         compiler_params=pltpu.CompilerParams(vmem_limit_bytes=52 << 20),
         name="attend",
-    )(numbers, z, cache, anc, wv)
+    )(numbers, z, keys, anc, wv)
 
 
 def combine_kernel(v_ref, o_ref):
@@ -696,7 +708,8 @@
     z = exchange(z, ALL)
     other = lax.ppermute(w_out, TP, [(n, n ^ 1) for n in range(8)])
     z, other = lax.optimization_barrier((z, other))
-    sent, fresh = attend(numbers, z, cache, anc, wv)
+    keys = own_keys(numbers, cache)
+    sent, fresh = attend(numbers, z, keys, anc, wv)
 
     updated = None
     for n in range(len(CUTS) - 1):
@@ -719,7 +732,7 @@
     return (result, jnp.transpose(updated, (0, 2, 1)))
 
 
-CUTS = (0, 5, 9, 24)
+CUTS = (0, 6, 11, 24)
 
 
 def solution(mesh):

time: 127 us -> 127 us (level)
  waiting for transfers between devices: 36.9 us -> 30.9 us
  Pallas kernels: 38.3 us -> 42.7 us
    all_to_all x6, waiting for transfers between devices: 36.9 us -> 30.9 us  [exchange(): return lax.all_to_all(value, axis, 0, 0, tiled=True)]
    pallas_call x0 -> x1, Pallas kernels: none -> 2.55 us  [own_keys(): pl.pallas_call(keys_kernel, out_shape=jax.ShapeDtypeStruct((3, LINES, SPA...]
    pallas_call x3, Pallas kernels: 21.7 us -> 23.1 us  [copy_cache(): pl.pallas_call(kernel, out_shape=jax.ShapeDtypeStruct(cache.shape, cache....]
  transfers between devices with their start and end apart: 13 -> 13, of which waited for: 5 -> 5; matrix products, arithmetic and copies ran while one was open for 4% -> 3% of each run, Pallas kernels for 23% -> 27%
where the time goes in v4:
time: 127 us; the launch traced here: 126 us
  starting transfers between devices  45.3 us (36%)
  Pallas kernels  42.7 us (34%)
  waiting for transfers between devices  30.9 us (24%)
  local copies, waits for them, and re-layouts  2.65 us (2%)
  other arithmetic  1.87 us (1%)
  matrix products  1.47 us (1%)
    all_to_all x6, starting transfers between devices, exchange(): return lax.all_to_all(value, axis, 0, 0, tiled=True)  37.6 us
    all_to_all x6, waiting for transfers between devices, exchange(): return lax.all_to_all(value, axis, 0, 0, tiled=True)  30.9 us
    pallas_call x3, Pallas kernels, copy_cache(): pl.pallas_call(kernel, out_shape=jax.ShapeDtypeStruct(cache.shape, cache....  23.1 us
    pallas_call x1, Pallas kernels, attend(): pl.pallas_call(attend_kernel, out_shape=(jax.ShapeDtypeStruct((16, 32, 12...  7.49 us
    ppermute x3, starting transfers between devices, layer(): lax.ppermute(mixed, 'y', [(n, (n + k) % 4) for n in range(4)])  5.09 us
    ppermute x3, starting transfers between devices, layer(): lax.ppermute(w_here[0], 'y', [(n, (n + k) % 4) for n in range(4)])  2.56 us
    pallas_call x1, Pallas kernels, own_keys(): pl.pallas_call(keys_kernel, out_shape=jax.ShapeDtypeStruct((3, LINES, SPA...  2.55 us
  transfers between devices with their start and end apart: 13, of which 5 were waited for; matrix products, arithmetic and copies ran while one was open for 3% of the time, Pallas kernels for 27%

profile of v4, /device:TPU:0, one launch (start us, length us, event | category | flops | bytes accessed | tf_op | source)
XLA Modules:
  0.0 125.9 jit_solution(8162406610529962570)
XLA Ops:
  0.7 1.9 %shard_map.149 = bf16[128,16,128]{2,1,0:T(8,128)(2,1)} custom-call(bf16[16,384]{1,0:T(8,128)(2,1)} %bitcast.46, bf16[16,512]{1,0:T(8,128)(2,1)} %q_ref.1, bf16[16,288]{1,0:T(8,128)(2,1)} %k_ref.1, bf16[1,16]{1,0:T(2,128)(2,1)} %bitcast.47), custom_call_target="tpu_custom_call" | custom-call | flops 100000000 | bytes 1000000 | tf_op jit(solution)/shard_map/pallas_call | solution.py:112
  2.6 11.3 %all-to-all-start = ((bf16[128,16,128]{2,1,0:T(8,128)(2,1)}), bf16[128,16,128]{2,1,0:T(8,128)(2,1)S(1)}, u32[]{:S(2)}, u32[]{:S(2)}) async-start(bf16[128,16,128]{2,1,0:T(8,128)(2,1)} %shard_map.149), calls=%async_computation | async-start | bytes 1048576 | tf_op jit(solution)/shard_map/all_to_all | solution.py:655
  13.9 0.8 copy.21
  16.4 0.7 add_convert_fusion
  17.3 0.7 bitcast_convert_fusion.gq_ref
  18.0 6.2 %copy_cache.3.refs_1_ = bf16[24,288,2048]{2,1,0:T(8,128)(2,1)} custom-call(bf16[24,288,2048]{2,1,0:T(8,128)(2,1)} %bitcast.37), custom_call_target="tpu_custom_call" | custom-call | flops 5400000000 | bytes 14155776 | tf_op jit(solution)/shard_map/copy_cache/pallas_call | solution.py:545
  24.2 3.1 %all-to-all-done = bf16[128,16,128]{2,1,0:T(8,128)(2,1)S(1)} async-done(((bf16[128,16,128]{2,1,0:T(8,128)(2,1)}), bf16[128,16,128]{2,1,0:T(8,128)(2,1)S(1)}, u32[]{:S(2)}, u32[]{:S(2)}) %all-to-all-start) | async-done | bytes 524320 | tf_op jit(solution)/shard_map/all_to_all | solution.py:655
  27.3 1.4 %shard_map.150 = f32[8,24,128]{2,1,0:T(8,128)} custom-call(bf16[2048,128]{1,0:T(8,128)(2,1)S(1)} %bitcast.32), custom_call_target="tpu_custom_call" | custom-call | flops 67108864 | bytes 524288 | tf_op jit(solution)/shard_map/pallas_call | solution.py:131
  28.7 3.4 %all-to-all-start.1 = ((f32[8,24,128]{2,1,0:T(8,128)}), f32[8,24,128]{2,1,0:T(8,128)S(1)}, u32[]{:S(2)}, u32[]{:S(2)}) async-start(f32[8,24,128]{2,1,0:T(8,128)} %shard_map.150), calls=%async_computation.1 | async-start | bytes 196608 | tf_op jit(solution)/shard_map/all_to_all | solution.py:655
  32.1 5.7 %all-to-all-done.1.y_ref = f32[8,24,128]{2,1,0:T(8,128)S(1)} async-done(((f32[8,24,128]{2,1,0:T(8,128)}), f32[8,24,128]{2,1,0:T(8,128)S(1)}, u32[]{:S(2)}, u32[]{:S(2)}) %all-to-all-start.1) | async-done | bytes 98336 | tf_op jit(solution)/shard_map/all_to_all | solution.py:655
  37.8 1.5 %queries.1 = bf16[128,24,128]{2,1,0:T(8,128)(2,1)} custom-call(s32[1]{0:T(128)} %bitcast.t_ref, f32[8,24,128]{2,1,0:T(8,128)S(1)} %all-to-all-done.1.y_ref, f32[4,128]{1,0:T(4,128)S(1)} %bitcast_convert_fusion.gq_ref, f32[2,128]{1,0:T(2,128)S(1)} %bitcast_convert_fusion.2.gk_ref, f32[24,128]{1,0:T(8,128)S(1)} %get-tuple-element.20.cos_ref, ...), custom_call_target="tpu_custom_call" | custom-call | flops 14155776 | bytes 786432 | tf_op jit(solution)/shard_map/queries/pallas_call | solution.py:209
  39.3 5.8 %all-to-all-start.2 = ((bf16[128,24,128]{2,1,0:T(8,128)(2,1)}), bf16[128,24,128]{2,1,0:T(8,128)(2,1)S(1)}, u32[]{:S(2)}, u32[]{:S(2)}) async-start(bf16[128,24,128]{2,1,0:T(8,128)(2,1)} %queries.1), calls=%async_computation.2 | async-start | bytes 1572864 | tf_op jit(solution)/shard_map/all_to_all | solution.py:655
  45.1 5.2 %copy_cache.4.refs_1_ = bf16[24,288,2048]{2,1,0:T(8,128)(2,1)} custom-call(bf16[24,288,2048]{2,1,0:T(8,128)(2,1)} %bitcast.38, bf16[24,288,2048]{2,1,0:T(8,128)(2,1)} %copy_cache.3.refs_1_), custom_call_target="tpu_custom_call", output_to_operand_aliasing={{}: (1, {})} | custom-call | flops 4499999744 | bytes 11796480 | tf_op jit(solution)/shard_map/copy_cache/pallas_call | solution.py:545
  50.4 2.5 %own_keys.1.keys = bf16[3,288,2048]{2,1,0:T(8,128)(2,1)S(1)} custom-call(s32[25]{0:T(128)S(1)} %pad_add_fusion.n_ref, bf16[24,288,2048]{2,1,0:T(8,128)(2,1)} %bitcast.39), custom_call_target="tpu_custom_call" | custom-call | flops 100000000 | bytes 7077888 | tf_op jit(solution)/shard_map/own_keys/pallas_call | solution.py:238
  53.0 1.7 %copy-done = bf16[3,288,2048]{2,1,0:T(8,128)(2,1)} copy-done((bf16[3,288,2048]{2,1,0:T(8,128)(2,1)}, bf16[3,288,2048]{2,1,0:T(8,128)(2,1)S(1)}, u32[]{:S(2)}) %copy-start) | copy-done | bytes 3538968
  54.7 6.6 %all-to-all-done.2.z_ref = bf16[128,24,128]{2,1,0:T(8,128)(2,1)S(1)} async-done(((bf16[128,24,128]{2,1,0:T(8,128)(2,1)}), bf16[128,24,128]{2,1,0:T(8,128)(2,1)S(1)}, u32[]{:S(2)}, u32[]{:S(2)}) %all-to-all-start.2) | async-done | bytes 786464 | tf_op jit(solution)/shard_map/all_to_all | solution.py:655
  61.3 7.5 %attend.1 = (bf16[16,32,128]{2,1,0:T(8,128)(2,1)}, bf16[24,16,384]{2,1,0:T(8,128)(2,1)S(1)}) custom-call(s32[25]{0:T(128)S(1)} %pad_add_fusion.n_ref, bf16[128,24,128]{2,1,0:T(8,128)(2,1)S(1)} %all-to-all-done.2.z_ref, bf16[3,288,2048]{2,1,0:T(8,128)(2,1)} %copy-done, f32[3,128,128]{2,1,0:T(8,128)S(1)} %broadcast_bitcast_fusion.anc_ref, ...), custom_call_target="tpu_custom_call" | custom-call | flops 1711276032 | bytes 3538944 | tf_op jit(solution)/shard_map/attend/pallas_call | solution.py:389
  68.8 3.5 %all-to-all-start.3 = ((bf16[16,32,128]{2,1,0:T(8,128)(2,1)}), bf16[16,32,128]{2,1,0:T(8,128)(2,1)S(1)}, u32[]{:S(2)}, u32[]{:S(2)}) async-start(bf16[16,32,128]{2,1,0:T(8,128)(2,1)} %get-tuple-element.9), calls=%async_computation.3 | async-start | bytes 262144 | tf_op jit(solution)/shard_map/all_to_all | solution.py:655
  72.4 11.7 %copy_cache.5.old_ref = bf16[24,288,2048]{2,1,0:T(8,128)(2,1)} custom-call(bf16[24,288,2048]{2,1,0:T(8,128)(2,1)} %bitcast.40, bf16[24,288,2048]{2,1,0:T(8,128)(2,1)} %copy_cache.4.refs_1_), custom_call_target="tpu_custom_call", output_to_operand_aliasing={{}: (1, {})} | custom-call | flops 11699999744 | bytes 30670848 | tf_op jit(solution)/shard_map/copy_cache/pallas_call | solution.py:545
  84.1 1.1 collective-permute-start.3
  85.2 1.5 %collective-permute-start.2 = (bf16[2,128,128]{2,1,0:T(8,128)(2,1)S(1)}, bf16[2,128,128]{2,1,0:T(8,128)(2,1)S(1)}, u32[]{:S(2)}, u32[]{:S(2)}) collective-permute-start(bf16[2,128,128]{2,1,0:T(8,128)(2,1)S(1)} %pad_maximum_fusion.refs_0_), channel_id=1, source_target_pairs={{0,4},{2,6},{4,0},{6,2},{1,5},{3,7},{5,1},{7,3},{8,12},{10,14},{12... | collective-permute-start | bytes 196616 | tf_op jit(solution)/shard_map/ppermute | solution.py:721
  86.7 1.0 shard_map.151
  87.7 7.4 %all-to-all-start.4 = ((bf16[32,24,128]{2,1,0:T(8,128)(2,1)}), bf16[32,24,128]{2,1,0:T(8,128)(2,1)S(1)}, u32[]{:S(2)}, u32[]{:S(2)}) async-start(bf16[32,24,128]{2,1,0:T(8,128)(2,1)} %shard_map.151), calls=%async_computation.4 | async-start | bytes 393216 | tf_op jit(solution)/shard_map/all_to_all | solution.py:655
  95.2 8.1 %all-to-all-done.4 = bf16[32,24,128]{2,1,0:T(8,128)(2,1)S(1)} async-done(((bf16[32,24,128]{2,1,0:T(8,128)(2,1)}), bf16[32,24,128]{2,1,0:T(8,128)(2,1)S(1)}, u32[]{:S(2)}, u32[]{:S(2)}) %all-to-all-start.4) | async-done | bytes 196640 | tf_op jit(solution)/shard_map/all_to_all | solution.py:655
  103.3 1.0 mix.1
  104.3 3.2 %collective-permute-start.6 = (f32[96,128]{1,0:T(8,128)S(1)}, f32[96,128]{1,0:T(8,128)S(1)}, u32[]{:S(2)}, u32[]{:S(2)}) collective-permute-start(f32[96,128]{1,0:T(8,128)S(1)} %get-tuple-element.12.refs_0_), channel_id=1, source_target_pairs={{0,6},{2,0},{4,2},{6,4},{1,7},{3,1},{5,3},{7,5},{8,14},{10,8},{12,... | collective-permute-start | bytes 147464 | tf_op jit(solution)/shard_map/ppermute | solution.py:729
  107.5 0.9 collective-permute-start.5
  108.4 1.0 collective-permute-start.4
  109.3 6.2 %all-to-all-start.5 = ((f32[64,1,128]{2,1,0:T(1,128)}), f32[64,1,128]{2,1,0:T(1,128)S(1)}, u32[]{:S(2)}, u32[]{:S(2)}) async-start(f32[64,1,128]{2,1,0:T(1,128)} %get-tuple-element.11), calls=%async_computation.5 | async-start | bytes 65536 | tf_op jit(solution)/shard_map/all_to_all | solution.py:655
  115.6 2.1 %place.1 = bf16[24,288,2048]{2,1,0:T(8,128)(2,1)} custom-call(s32[25]{0:T(128)S(1)} %pad_add_fusion.n_ref, bf16[24,288,2048]{2,1,0:T(8,128)(2,1)} %bitcast.41, bf16[24,16,384]{2,1,0:T(8,128)(2,1)S(1)} %get-tuple-element.13.fresh_ref, bf16[24,288,2048]{2,1,0:T(8,128)(2,1)} %copy_cache.5.old_ref), custom_call_target="tpu_custom_call", output_to_operand_aliasing={{}: (3, {})} | custom-call | flops 1000000000 | bytes 2000000 | tf_op jit(solution)/shard_map/place/pallas_call | solution.py:623
  117.6 7.4 %all-to-all-done.5 = f32[64,1,128]{2,1,0:T(1,128)S(1)} async-done(((f32[64,1,128]{2,1,0:T(1,128)}), f32[64,1,128]{2,1,0:T(1,128)S(1)}, u32[]{:S(2)}, u32[]{:S(2)}) %all-to-all-start.5) | async-done | bytes 32800 | tf_op jit(solution)/shard_map/all_to_all | solution.py:655
  125.1 0.8 finish.1
  (39 shorter events, 2.2 us)
Async XLA Ops:
  0.6 54.1 %collective-permute-start = (bf16[128,128]{1,0:T(8,128)(2,1)}, bf16[128,128]{1,0:T(8,128)(2,1)S(1)}, u32[]{:S(2)}, u32[]{:S(2)}) collective-permute-start(bf16[128,128]{1,0:T(8,128)(2,1)} %param.26), channel_id=1, source_target_pairs={{0,1},{1,0},{2,3},{3,2},{4,5},{5,4},{6,7},{7,6},{8,9},{9,8},{10,11... | collective-permute-start | bytes 98312 | tf_op jit(solution)/shard_map/ppermute | solution.py:709
  2.6 24.8 %all-to-all-start = ((bf16[128,16,128]{2,1,0:T(8,128)(2,1)}), bf16[128,16,128]{2,1,0:T(8,128)(2,1)S(1)}, u32[]{:S(2)}, u32[]{:S(2)}) async-start(bf16[128,16,128]{2,1,0:T(8,128)(2,1)} %shard_map.149), calls=%async_computation | async-start | bytes 1048576 | tf_op jit(solution)/shard_map/all_to_all | solution.py:655
  18.0 14.1 %copy-start.4 = (bf16[256]{0:T(256)(128)(2,1)S(1)}, bf16[256]{0:T(256)(128)(2,1)}, u32[]{:S(2)}) copy-start(bf16[256]{0:T(256)(128)(2,1)} %param.23) | copy-start | bytes 1540
  18.0 19.8 %copy-start.1 = (bf16[512,2,288]{0,2,1:T(8,128)(2,1)S(1)}, bf16[512,2,288]{0,2,1:T(8,128)(2,1)}, u32[]{:S(2)}) copy-start(bf16[512,2,288]{0,2,1:T(8,128)(2,1)} %param.24) | copy-start | bytes 1769476
  28.7 9.1 %all-to-all-start.1 = ((f32[8,24,128]{2,1,0:T(8,128)}), f32[8,24,128]{2,1,0:T(8,128)S(1)}, u32[]{:S(2)}, u32[]{:S(2)}) async-start(f32[8,24,128]{2,1,0:T(8,128)} %shard_map.150), calls=%async_computation.1 | async-start | bytes 196608 | tf_op jit(solution)/shard_map/all_to_all | solution.py:655
  39.3 22.1 %all-to-all-start.2 = ((bf16[128,24,128]{2,1,0:T(8,128)(2,1)}), bf16[128,24,128]{2,1,0:T(8,128)(2,1)S(1)}, u32[]{:S(2)}, u32[]{:S(2)}) async-start(bf16[128,24,128]{2,1,0:T(8,128)(2,1)} %queries.1), calls=%async_computation.2 | async-start | bytes 1572864 | tf_op jit(solution)/shard_map/all_to_all | solution.py:655
  50.3 11.0 %copy-start.2 = (bf16[16,256,64]{1,2,0:T(8,128)(2,1)S(1)}, bf16[16,256,64]{1,2,0:T(8,128)(2,1)}, u32[]{:S(2)}) copy-start(bf16[16,256,64]{1,2,0:T(8,128)(2,1)} %param.25) | copy-start | bytes 1572868
  53.0 1.8 %copy-start = (bf16[3,288,2048]{2,1,0:T(8,128)(2,1)}, bf16[3,288,2048]{2,1,0:T(8,128)(2,1)S(1)}, u32[]{:S(2)}) copy-start(bf16[3,288,2048]{2,1,0:T(8,128)(2,1)S(1)} %own_keys.1.keys) | copy-start | bytes 10616836
  68.8 17.9 %all-to-all-start.3 = ((bf16[16,32,128]{2,1,0:T(8,128)(2,1)}), bf16[16,32,128]{2,1,0:T(8,128)(2,1)S(1)}, u32[]{:S(2)}, u32[]{:S(2)}) async-start(bf16[16,32,128]{2,1,0:T(8,128)(2,1)} %get-tuple-element.9), calls=%async_computation.3 | async-start | bytes 262144 | tf_op jit(solution)/shard_map/all_to_all | solution.py:655
  72.3 11.7 %copy-start.3 = (bf16[128,128]{1,0:T(8,128)(2,1)S(1)}, bf16[128,128]{1,0:T(8,128)(2,1)}, u32[]{:S(2)}) copy-start(bf16[128,128]{1,0:T(8,128)(2,1)} %param.26) | copy-start | bytes 98308
  72.3 22.8 %copy-start.5 = (bf16[128]{0:T(256)(128)(2,1)S(1)}, bf16[128]{0:T(256)(128)(2,1)}, u32[]{:S(2)}) copy-start(bf16[128]{0:T(256)(128)(2,1)} %param.27) | copy-start | bytes 772
  84.1 11.0 %collective-permute-start.3 = (bf16[2,128,128]{2,1,0:T(8,128)(2,1)S(1)}, bf16[2,128,128]{2,1,0:T(8,128)(2,1)S(1)}, u32[]{:S(2)}, u32[]{:S(2)}) collective-permute-start(bf16[2,128,128]{2,1,0:T(8,128)(2,1)S(1)} %pad_maximum_fusion.refs_0_), channel_id=1, source_target_pairs={{0,6},{2,0},{4,2},{6,4},{1,7},{3,1},{5,3},{7,5},{8,14},{10,8},{12,... | collective-permute-start | bytes 196616 | tf_op jit(solution)/shard_map/ppermute | solution.py:721
  85.2 10.0 %collective-permute-start.2 = (bf16[2,128,128]{2,1,0:T(8,128)(2,1)S(1)}, bf16[2,128,128]{2,1,0:T(8,128)(2,1)S(1)}, u32[]{:S(2)}, u32[]{:S(2)}) collective-permute-start(bf16[2,128,128]{2,1,0:T(8,128)(2,1)S(1)} %pad_maximum_fusion.refs_0_), channel_id=1, source_target_pairs={{0,4},{2,6},{4,0},{6,2},{1,5},{3,7},{5,1},{7,3},{8,12},{10,14},{12... | collective-permute-start | bytes 196616 | tf_op jit(solution)/shard_map/ppermute | solution.py:721
  86.7 8.5 %collective-permute-start.1 = (bf16[2,128,128]{2,1,0:T(8,128)(2,1)S(1)}, bf16[2,128,128]{2,1,0:T(8,128)(2,1)S(1)}, u32[]{:S(2)}, u32[]{:S(2)}) collective-permute-start(bf16[2,128,128]{2,1,0:T(8,128)(2,1)S(1)} %pad_maximum_fusion.refs_0_), channel_id=1, source_target_pairs={{0,2},{2,4},{4,6},{6,0},{1,3},{3,5},{5,7},{7,1},{8,10},{10,12},{12... | collective-permute-start | bytes 196616 | tf_op jit(solution)/shard_map/ppermute | solution.py:721
  87.7 15.6 %all-to-all-start.4 = ((bf16[32,24,128]{2,1,0:T(8,128)(2,1)}), bf16[32,24,128]{2,1,0:T(8,128)(2,1)S(1)}, u32[]{:S(2)}, u32[]{:S(2)}) async-start(bf16[32,24,128]{2,1,0:T(8,128)(2,1)} %shard_map.151), calls=%async_computation.4 | async-start | bytes 393216 | tf_op jit(solution)/shard_map/all_to_all | solution.py:655
  104.3 20.8 %collective-permute-start.6 = (f32[96,128]{1,0:T(8,128)S(1)}, f32[96,128]{1,0:T(8,128)S(1)}, u32[]{:S(2)}, u32[]{:S(2)}) collective-permute-start(f32[96,128]{1,0:T(8,128)S(1)} %get-tuple-element.12.refs_0_), channel_id=1, source_target_pairs={{0,6},{2,0},{4,2},{6,4},{1,7},{3,1},{5,3},{7,5},{8,14},{10,8},{12,... | collective-permute-start | bytes 147464 | tf_op jit(solution)/shard_map/ppermute | solution.py:729
  107.5 17.6 %collective-permute-start.5 = (f32[96,128]{1,0:T(8,128)S(1)}, f32[96,128]{1,0:T(8,128)S(1)}, u32[]{:S(2)}, u32[]{:S(2)}) collective-permute-start(f32[96,128]{1,0:T(8,128)S(1)} %get-tuple-element.12.refs_0_), channel_id=1, source_target_pairs={{0,4},{2,6},{4,0},{6,2},{1,5},{3,7},{5,1},{7,3},{8,12},{10,14},{12... | collective-permute-start | bytes 147464 | tf_op jit(solution)/shard_map/ppermute | solution.py:729
  108.4 16.7 %collective-permute-start.4 = (f32[96,128]{1,0:T(8,128)S(1)}, f32[96,128]{1,0:T(8,128)S(1)}, u32[]{:S(2)}, u32[]{:S(2)}) collective-permute-start(f32[96,128]{1,0:T(8,128)S(1)} %get-tuple-element.12.refs_0_), channel_id=1, source_target_pairs={{0,2},{2,4},{4,6},{6,0},{1,3},{3,5},{5,7},{7,1},{8,10},{10,12},{12... | collective-permute-start | bytes 147464 | tf_op jit(solution)/shard_map/ppermute | solution.py:729
  109.3 15.7 %all-to-all-start.5 = ((f32[64,1,128]{2,1,0:T(1,128)}), f32[64,1,128]{2,1,0:T(1,128)S(1)}, u32[]{:S(2)}, u32[]{:S(2)}) async-start(f32[64,1,128]{2,1,0:T(1,128)} %get-tuple-element.11), calls=%async_computation.5 | async-start | bytes 65536 | tf_op jit(solution)/shard_map/all_to_all | solution.py:655
